TPU v7x, 128 devices: a whole 4x4x4 slice. The times are simulated.
128 devices in a mesh: kv: 16 (over z, x), tp: 8 (over y, core).
Axes of the slice: x: 4, y: 4, z: 4, core: 2. Of those that a mesh axis runs over, the one named last changes fastest.
Arguments:
- tokens: bfloat16 [32768, 2048], P('kv'), may hold values from -6 to 6
- norm_gain: bfloat16 [2048], replicated, may hold values from 0.099609375 to 1.8984375
- query_weight: bfloat16 [2048, 1024], P(None, 'tp'), may hold values from -0.125 to 0.125
- cmp_key_weight: bfloat16 [2048, 512], P(None, 'tp'), may hold values from -0.125 to 0.125
- cmp_value_weight: bfloat16 [2048, 512], P(None, 'tp'), may hold values from -0.125 to 0.125
- sel_key_weight: bfloat16 [2048, 512], P(None, 'tp'), may hold values from -0.125 to 0.125
- sel_value_weight: bfloat16 [2048, 512], P(None, 'tp'), may hold values from -0.125 to 0.125
- branch_weight: bfloat16 [2, 2048, 16], replicated, may hold values from -0.125 to 0.125
- key_embed: bfloat16 [8, 32, 64], P('tp'), may hold values from -3 to 3
- key_inner: bfloat16 [8, 2048, 64], P('tp'), may hold values from -0.125 to 0.125
- key_outer: bfloat16 [8, 64, 64], P('tp'), may hold values from -0.75 to 0.75
- value_embed: bfloat16 [8, 32, 64], P('tp'), may hold values from -3 to 3
- value_inner: bfloat16 [8, 2048, 64], P('tp'), may hold values from -0.125 to 0.125
- value_outer: bfloat16 [8, 64, 64], P('tp'), may hold values from -0.75 to 0.75
- out_weight: bfloat16 [1024, 2048], replicated, may hold values from -0.1875 to 0.1875
- chosen: int32 [8, 256, 8], P('tp'), may hold values from 0 to 511, as said below
Outputs:
- attended: bfloat16 [32768, 2048], P(('kv', 'tp'))
Inputs may be any that keep to these rules, and one draw needn't show every extreme that they name: `chosen`: each entry is the index of a block of 64 positions in the whole sequence. For every key head and query block, its 8 entries lie in 8 different aligned spans of 2048 positions (at most one from any span), and none lies inside the query block's own positions.
All inputs are finite; a program needn't handle non-finite values.
Results may differ from a plain program's by a relative error of at most 0.0075.
Values may be sent and summed in bfloat16 or wider, within the bound.
No kernel may reach another device: no remote copies, remote signals or barrier semaphores. Data moves between devices by JAX's collectives and lax.ppermute only.
A program may use at most 128 MiB of HBM per device.

v0:
```python
import jax
import jax.numpy as jnp
from jax import lax
from jax.sharding import PartitionSpec as P

HEAD_DIM = 64
CMP_BLOCK = 32
SEL_BLOCK = 64
Q_BLOCK = 128
FAR_PICKS = 8


ROPE_BASE = 10000.0
norm_eps = 1e-06
masked_score = -1000000000.0


def copy_for_each(x, axis):
    peers = lax.axis_size(axis)
    return lax.all_to_all(jnp.broadcast_to(x[None], (peers, *x.shape)), axis, 0, 0, tiled=True)


def in_order(pieces, dim):
    shape = list(pieces.shape[1:])
    shape[dim] *= pieces.shape[0]
    return jnp.moveaxis(pieces, 0, dim).reshape(shape)


def collect(x, axis, dim):
    pieces = copy_for_each(x, axis)
    return in_order(pieces, dim)


def rotate(values_in, positions):
    half_dim = values_in.shape[-1] // 2
    inverse = ROPE_BASE ** (-jnp.arange(half_dim, dtype=jnp.float32) / half_dim)
    rotary_phases = positions.astype(jnp.float32)[:, None] * inverse[None, :]
    cosine = jnp.cos(rotary_phases)[:, None, :]
    sine = jnp.sin(rotary_phases)[:, None, :]
    first_half = values_in[..., :half_dim]
    second_half = values_in[..., half_dim:]
    return jnp.concatenate(
        [first_half * cosine - second_half * sine, second_half * cosine + first_half * sine],
        axis=-1,
    )


def summarize(raw_rows, embed, inner, outer):
    kv_local = embed.shape[0]
    block_count = raw_rows.shape[0] // CMP_BLOCK
    blocked = (
        raw_rows.reshape(block_count, CMP_BLOCK, kv_local, HEAD_DIM)
        .transpose(2, 0, 1, 3)
        .astype(jnp.float32)
    )
    blocked = (blocked + embed.astype(jnp.float32)[:, None]).astype(jnp.bfloat16)
    blocked = blocked.reshape(kv_local, block_count, CMP_BLOCK * HEAD_DIM)
    hidden = jax.nn.gelu(
        jnp.einsum("knc,kce->kne", blocked, inner, preferred_element_type=jnp.float32)
    ).astype(jnp.bfloat16)
    return jnp.einsum("kne,kef->knf", hidden, outer, preferred_element_type=jnp.float32).astype(
        jnp.bfloat16
    )


def per_device(
    tokens,
    norm_gain,
    query_weight,
    cmp_key_weight,
    cmp_value_weight,
    sel_key_weight,
    sel_value_weight,
    branch_weight,
    key_embed,
    key_inner,
    key_outer,
    value_embed,
    value_inner,
    value_outer,
    out_weight,
    chosen,
):
    tok_rows = tokens.shape[0]
    kv_local = key_embed.shape[0]
    heads_local = query_weight.shape[1] // HEAD_DIM
    group_size = heads_local // kv_local
    owners = lax.axis_size("kv")
    dev_index = lax.axis_index("kv")
    offset = dev_index * tok_rows
    positions = offset + jnp.arange(tok_rows, dtype=jnp.int32)
    scale = HEAD_DIM ** (-0.5)
    expanded_mask = tokens.astype(jnp.float32)
    normed = (
        expanded_mask
        * lax.rsqrt(jnp.mean(expanded_mask * expanded_mask, axis=-1, keepdims=True) + norm_eps)
        * norm_gain.astype(jnp.float32)
    ).astype(jnp.bfloat16)
    gate_cols = lax.dynamic_slice_in_dim(
        branch_weight, lax.axis_index("tp") * heads_local, heads_local, 2
    )
    q_width = heads_local * HEAD_DIM
    kv_width = kv_local * HEAD_DIM
    joined_weight = jnp.concatenate(
        [
            query_weight,
            cmp_key_weight,
            cmp_value_weight,
            sel_key_weight,
            sel_value_weight,
            gate_cols[0],
            gate_cols[1],
        ],
        axis=1,
    )
    projected = jnp.dot(normed, joined_weight, preferred_element_type=jnp.float32)
    bounds = [
        q_width,
        q_width + kv_width,
        q_width + 2 * kv_width,
        q_width + 3 * kv_width,
        q_width + 4 * kv_width,
        q_width + 4 * kv_width + heads_local,
    ]
    (
        query_part,
        cmp_key_part,
        cmp_value_part,
        sel_key_part,
        sel_value_part,
        gate_cmp_part,
        gate_sel_part,
    ) = jnp.split(projected, bounds, axis=1)
    query = query_part.reshape(tok_rows, heads_local, HEAD_DIM)
    q_plain = query.astype(jnp.bfloat16)
    q_turn = rotate(query, positions).astype(jnp.bfloat16)
    cmp_key = cmp_key_part.astype(jnp.bfloat16).reshape(tok_rows, kv_local, HEAD_DIM)
    cmp_value = cmp_value_part.astype(jnp.bfloat16).reshape(tok_rows, kv_local, HEAD_DIM)
    sel_key = rotate(sel_key_part.reshape(tok_rows, kv_local, HEAD_DIM), positions).astype(
        jnp.bfloat16
    )
    selected_value = sel_value_part.astype(jnp.bfloat16).reshape(tok_rows, kv_local, HEAD_DIM)
    gate_cmp = jax.nn.sigmoid(gate_cmp_part)
    gate_sel = jax.nn.sigmoid(gate_sel_part)
    summary = jnp.concatenate(
        [
            summarize(cmp_key, key_embed, key_inner, key_outer),
            summarize(cmp_value, value_embed, value_inner, value_outer),
        ],
        axis=-1,
    )
    summaries = collect(summary, "kv", 1)
    summary_count = summaries.shape[1]
    block_end = (jnp.arange(summary_count, dtype=jnp.int32) + 1) * CMP_BLOCK - 1
    q_group = q_plain.reshape(tok_rows, kv_local, group_size, HEAD_DIM).transpose(1, 0, 2, 3)
    cmp_scores = (
        jnp.einsum(
            "ktgd,kcd->ktgc", q_group, summaries[..., :HEAD_DIM], preferred_element_type=jnp.float32
        )
        * scale
    )
    usable = (block_end[None, :] <= positions[:, None])[None, :, None, :]
    cmp_probs = jax.nn.softmax(
        jnp.where(usable, cmp_scores, masked_score), axis=-1
    ) * usable.astype(jnp.float32)
    out_cmp = jnp.einsum(
        "ktgc,kcd->ktgd",
        cmp_probs.astype(jnp.bfloat16),
        summaries[..., HEAD_DIM:],
        preferred_element_type=jnp.float32,
    )
    out_cmp = out_cmp.transpose(1, 0, 2, 3).reshape(tok_rows, heads_local, HEAD_DIM)
    span_queries = tok_rows // Q_BLOCK
    span_blocks = tok_rows // SEL_BLOCK
    kv_sel = jnp.concatenate([sel_key, selected_value], axis=-1).transpose(1, 0, 2)
    all_picks = chosen.reshape(kv_local, owners, span_queries, FAR_PICKS)
    my_picks = lax.dynamic_index_in_dim(all_picks, dev_index, 1, keepdims=False)
    head_lane = jnp.arange(kv_local, dtype=jnp.int32)[:, None, None]
    matches = all_picks // span_blocks == dev_index
    wanted = jnp.sum(jnp.where(matches, all_picks % span_blocks, 0), axis=3)
    blocked = kv_sel.reshape(kv_local, span_blocks, SEL_BLOCK, 2 * HEAD_DIM)
    outgoing = blocked[head_lane, wanted]
    incoming = lax.all_to_all(outgoing, "kv", split_axis=1, concat_axis=1, tiled=True)
    source = my_picks // span_blocks
    query_lane = jnp.arange(span_queries, dtype=jnp.int32)[None, :, None]
    picked = incoming[head_lane, source, query_lane]
    own_keys = kv_sel.reshape(kv_local, span_queries, Q_BLOCK, 2 * HEAD_DIM)
    keys_all = jnp.concatenate(
        [own_keys, picked.reshape(kv_local, span_queries, FAR_PICKS * SEL_BLOCK, 2 * HEAD_DIM)],
        axis=2,
    )
    query_pos = positions.reshape(span_queries, Q_BLOCK)
    far_pos = (my_picks[..., None] * SEL_BLOCK + jnp.arange(SEL_BLOCK, dtype=jnp.int32)).reshape(
        kv_local, span_queries, FAR_PICKS * SEL_BLOCK
    )
    key_pos = jnp.concatenate([query_pos[None], far_pos], axis=2)
    q_sel = q_turn.reshape(span_queries, Q_BLOCK, kv_local, group_size, HEAD_DIM).transpose(
        2, 0, 1, 3, 4
    )
    sel_scores = (
        jnp.einsum(
            "knqgd,knmd->knqgm", q_sel, keys_all[..., :HEAD_DIM], preferred_element_type=jnp.float32
        )
        * scale
    )
    allowed_keys = key_pos[:, :, None, None, :] <= query_pos[None, :, :, None, None]
    sel_probs = jax.nn.softmax(jnp.where(allowed_keys, sel_scores, masked_score), axis=-1)
    out_sel = jnp.einsum(
        "knqgm,knmd->knqgd",
        sel_probs.astype(jnp.bfloat16),
        keys_all[..., HEAD_DIM:],
        preferred_element_type=jnp.float32,
    )
    out_sel = out_sel.transpose(1, 2, 0, 3, 4).reshape(tok_rows, heads_local, HEAD_DIM)
    mixed = (
        (gate_cmp[..., None] * out_cmp + gate_sel[..., None] * out_sel)
        .reshape(tok_rows, heads_local * HEAD_DIM)
        .astype(jnp.bfloat16)
    )
    head_rows = lax.all_to_all(mixed, "tp", split_axis=0, concat_axis=1, tiled=True)
    return jnp.dot(head_rows, out_weight, preferred_element_type=jnp.float32).astype(jnp.bfloat16)


def solution(mesh):
    placed = (
        P("kv", None),
        P(),
        P(None, "tp"),
        P(None, "tp"),
        P(None, "tp"),
        P(None, "tp"),
        P(None, "tp"),
        P(),
        P("tp", None, None),
        P("tp", None, None),
        P("tp", None, None),
        P("tp", None, None),
        P("tp", None, None),
        P("tp", None, None),
        P(),
        P("tp", None, None),
    )
    return jax.shard_map(
        per_device, mesh=mesh, in_specs=placed, out_specs=P(("kv", "tp"), None), check_vma=False
    )
```

profile of v0, /device:TPU:1, one launch (start us, length us, event | category | flops | bytes accessed | tf_op | source)
XLA Modules:
  0.0 171.9 jit_solution(5051237416359795915)
XLA Ops:
  0.8 5.1 %fusion.2 = f32[2048]{0:T(1024)S(1)} fusion(bf16[2048,2048]{1,0:T(8,128)(2,1)} %param.16), kind=kLoop, calls=%fused_computation.6 | loop fusion | flops 12580864 | bytes 8396800 | tf_op jit(solution)/shard_map/reduce_sum | solution.py:96
  12.4 5.5 %concatenate.68 = bf16[2048,388]{1,0:T(8,128)(2,1)} concatenate(bf16[2048,128]{1,0:T(8,128)(2,1)} %param.18, bf16[2048,64]{1,0:T(8,128)(2,1)} %copy.58, bf16[2048,64]{1,0:T(8,128)(2,1)} %copy.59, bf16[2048,64]{1,0:T(8,128)(2,1)} %copy.60, bf16[2048,64]{1,0:T(8,128)(2,1)} %copy.61, bf16[2048,2]{1,0:T(8,128)(2,1)S(1)} %copy.62, bf16[2048,2]{1,0:T(8,128)(2,1)S(1)} %copy.63), dimensions={1} | concatenate | bytes 3178496 | tf_op jit(solution)/shard_map/concatenate | solution.py:104
  17.8 9.4 %fusion.119 = (bf16[2048,388]{0,1:T(8,128)(2,1)S(1)}, f32[2048,388]{0,1:T(8,128)}) fusion(bf16[2048,388]{1,0:T(8,128)(2,1)} %concatenate.68, bf16[2048,2048]{1,0:T(8,128)(2,1)} %param.16, f32[2048]{0:T(1024)S(1)} %convert_element_type.126, f32[2048]{0:T(1024)S(1)} %add_rsqrt_fusion), kind=kOutput, calls=%fused_computation.179 | convolution fusion | flops 3272351744 | bytes 14761984 | tf_op jit(solution)/shard_map/dot_general | solution.py:116
  31.5 8.5 %all-to-all-start = ((bf16[16,1,64,128]{3,2,1,0:T(8,128)(2,1)}), bf16[16,1,64,128]{3,2,1,0:T(8,128)(2,1)}, u32[]{:S(2)}, u32[]{:S(2)}) async-start(bf16[16,1,64,128]{3,2,1,0:T(8,128)(2,1)} %broadcast_in_dim.34), calls=%async_computation | async-start | bytes 524288 | tf_op jit(solution)/shard_map/all_to_all | solution.py:20
  40.2 1.7 %slice_bitcast_fusion.14 = (bf16[8,8,16,128]{3,1,2,0:T(8,128)(2,1)}, bf16[2048,64]{0,1:T(8,128)(2,1)S(1)}) fusion(bf16[2048,388]{0,1:T(8,128)(2,1)} %copy-done.11), kind=kLoop, calls=%fused_computation.176 | loop fusion | bytes 786432
  46.7 1.8 %multiply_cosine_fusion.1 = (f32[2048,32]{0,1:T(8,128)}, f32[2048,32]{0,1:T(8,128)}) fusion(f32[32]{0:T(128)S(1)} %multiply_power_fusion, f32[2048]{0:T(1024)S(1)} %get-tuple-element.30), kind=kLoop, calls=%fused_computation.56 | loop fusion | flops 65536 | bytes 532608 | tf_op jit(solution)/shard_map/cos | solution.py:38
  50.3 1.8 %broadcast_compare_fusion.1 = pred[16,128,640]{2,1,0:T(8,128)(4,1)} fusion(s32[16,128]{1,0:T(8,128)S(1)} %add_add_fusion, s32[16,640]{1,0:T(8,128)S(1)} %add_bitcast_fusion), kind=kLoop, calls=%fused_computation.30 | loop fusion | flops 1310720 | bytes 1359872 | tf_op jit(solution)/shard_map/le | solution.py:206
  52.5 3.1 %gather_fusion = bf16[256,64,128]{2,1,0:T(8,128)(2,1)} fusion(bf16[1,32,64,128]{3,2,1,0:T(8,128)(2,1)S(1)} %pad_maximum_fusion.1, s32[256]{0:T(256)S(1)} %reshape.731), kind=kCustom, calls=%fused_computation | custom fusion | bytes 8390656 | tf_op jit(solution)/shard_map/gather | solution.py:182
  55.8 6.8 %all-to-all-start.1 = ((bf16[1,16,16,64,128]{4,3,2,0,1:T(8,128)(2,1)}), bf16[1,16,16,64,128]{4,3,2,0,1:T(8,128)(2,1)}, u32[]{:S(2)}, u32[]{:S(2)}) async-start(bf16[1,16,16,64,128]{4,3,2,0,1:T(8,128)(2,1)} %bitcast.158), calls=%async_computation.1 | async-start | bytes 8388608 | tf_op jit(solution)/shard_map/all_to_all | solution.py:183
  62.6 2.1 %split.57 = bf16[2048,128]{0,1:T(8,128)(2,1)} slice(f32[2048,388]{0,1:T(8,128)} %get-tuple-element.24), slice={[0:2048], [0:128]} | slice | bytes 1048576 | tf_op jit(solution)/shard_map/split | solution.py:133
  68.5 4.2 %fusion.118 = (f32[2048,1024]{0,1:T(8,128)}, pred[2048,1024]{0,1:T(8,128)(4,1)S(1)}) fusion(s32[2048]{0:T(1024)S(1)} %get-tuple-element.29, s32[1024]{0:T(1024)S(1)} %multiply_add_fusion), kind=kLoop, calls=%fused_computation.178 | loop fusion | flops 4194304 | bytes 10498048 | tf_op jit(solution)/shard_map/convert_element_type | solution.py:165
  72.6 10.6 %fusion.121 = (f32[2048,2]{0,1:T(2,128)S(1)}, f32[2048,2,1024]{0,2,1:T(8,128)}) fusion(pred[2048,1024]{0,1:T(8,128)(4,1)S(1)} %get-tuple-element.20, bf16[2048,2,64]{0,2,1:T(8,128)(2,1)} %bitcast.173, bf16[1,1024,128]{2,1,0:T(8,128)(2,1)} %bitcast.14), kind=kOutput, calls=%fused_computation.181 | convolution fusion | flops 553649152 | bytes 19677184 | tf_op jit(solution)/shard_map/sub | solution.py:163
  83.3 9.4 %fusion.19 = f32[2048,2,64]{0,2,1:T(8,128)S(1)} fusion(f32[2048,2,1024]{0,2,1:T(8,128)} %get-tuple-element.28, f32[2048,1024]{0,1:T(8,128)} %get-tuple-element.19, f32[2048,2]{0,1:T(2,128)S(1)} %get-tuple-element.27, f32[2048,2]{0,1:T(2,128)S(1)} %copy-done.20, bf16[1,1024,128]{2,1,0:T(8,128)(2,1)} %bitcast.14), kind=kOutput, calls=%fused_computation.32 | convolution fusion | flops 549715968 | bytes 26509312 | tf_op jit(solution)/shard_map/ktgc,kcd->ktgd/dot_general | solution.py:166
  94.0 29.5 %all-to-all-done.1 = bf16[1,16,16,64,128]{4,3,2,0,1:T(8,128)(2,1)} async-done(((bf16[1,16,16,64,128]{4,3,2,0,1:T(8,128)(2,1)}), bf16[1,16,16,64,128]{4,3,2,0,1:T(8,128)(2,1)}, u32[]{:S(2)}, u32[]{:S(2)}) %all-to-all-start.1) | async-done | bytes 4194336 | tf_op jit(solution)/shard_map/all_to_all | solution.py:183
  123.5 4.5 %gather_fusion.1 = bf16[128,64,128]{2,1,0:T(8,128)(2,1)} fusion(bf16[1,16,16,64,128]{4,3,2,1,0:T(8,128)(2,1)} %bitcast.29, s32[128]{0:T(128)S(1)} %reshape.739), kind=kCustom, calls=%fused_computation.1 | custom fusion | bytes 4195840 | tf_op jit(solution)/shard_map/gather | solution.py:186
  127.9 2.9 %copy.83 = bf16[1,16,512,128]{2,3,1,0:T(8,128)(2,1)S(1)} copy(bf16[1,16,512,128]{3,2,1,0:T(8,128)(2,1)} %bitcast.159) | data formatting | bytes 4194304 | tf_op jit(solution)/shard_map/reshape | solution.py:189
  132.2 1.6 copy-done.2
  133.8 1.6 fusion.22
  135.4 7.2 %fusion.120 = (f32[16,128,2]{1,2,0:T(2,128)S(1)}, f32[16,128,2,640]{3,1,2,0:T(8,128)}) fusion(f32[16,128,2,640]{3,1,2,0:T(8,128)S(1)} %fusion.22, pred[16,128,640]{2,1,0:T(8,128)(4,1)S(1)} %copy-done.5), kind=kOutput, calls=%fused_computation.180 | output fusion | flops 15729279 | bytes 22298624 | tf_op jit(solution)/shard_map/sub | solution.py:207
  142.5 5.4 %fusion.18 = f32[16,128,2,64]{1,3,2,0:T(8,128)S(1)} fusion(f32[16,128,2,640]{3,1,2,0:T(8,128)} %get-tuple-element.26, f32[16,128,2]{1,2,0:T(2,128)S(1)} %get-tuple-element.25, bf16[1,16,640,128]{2,3,1,0:T(8,128)(2,1)S(1)} %copy-done.3), kind=kOutput, calls=%fused_computation.27 | convolution fusion | flops 340787200 | bytes 12861440 | tf_op jit(solution)/shard_map/knqgm,knmd->knqgd/dot_general | solution.py:208
  148.0 1.6 copy.84
  149.5 2.5 %reshape_transpose.10 = f32[8,256,128]{1,0,2:T(8,128)} reshape(f32[16,128,2,64]{1,0,3,2:T(8,128)} %copy.84) | data formatting | bytes 2097152 | tf_op jit(solution)/shard_map/reshape;transpose | solution.py:214
  153.7 15.9 %all_to_all.26 = bf16[8,256,128]{1,2,0:T(8,128)(2,1)S(1)} all-to-all(bf16[8,256,128]{1,2,0:T(8,128)(2,1)S(1)} %copy.85), channel_id=1, replica_groups=mesh['kv'=16,'tp'=8] {'tp'}, dimensions={0} | all-to-all | bytes 1048576 | tf_op jit(solution)/shard_map/all_to_all | solution.py:220
  169.6 2.2 %convolution_convert_fusion = bf16[256,2048]{1,0:T(8,128)(2,1)} fusion(bf16[256,1024]{0,1:T(8,128)(2,1)S(1)} %bitcast.174, bf16[1024,2048]{1,0:T(8,128)(2,1)S(1)} %copy-done.23), kind=kOutput, calls=%fused_computation.31 | convolution fusion | flops 1074266112 | bytes 5767168 | tf_op jit(solution)/shard_map/dot_general | solution.py:221
  (122 shorter events, 26.6 us)
Async XLA Ops:
  0.0 29.9 %copy-start = (bf16[1,2048,64]{1,2,0:T(8,128)(2,1)S(1)}, bf16[1,2048,64]{1,2,0:T(8,128)(2,1)}, u32[]{:S(2)}) copy-start(bf16[1,2048,64]{1,2,0:T(8,128)(2,1)} %param.25) | copy-start | bytes 786436
  0.0 5.9 %copy-start.21 = (bf16[1,32,64]{2,1,0:T(8,128)(2,1)S(1)}, bf16[1,32,64]{2,1,0:T(8,128)(2,1)}, u32[]{:S(2)}) copy-start(bf16[1,32,64]{2,1,0:T(8,128)(2,1)} %param.24) | copy-start | bytes 12292
  0.0 6.0 %copy-start.22 = (bf16[1,32,64]{2,1,0:T(8,128)(2,1)S(1)}, bf16[1,32,64]{2,1,0:T(8,128)(2,1)}, u32[]{:S(2)}) copy-start(bf16[1,32,64]{2,1,0:T(8,128)(2,1)} %param.27) | copy-start | bytes 12292
  0.0 7.4 %copy-start.12 = (bf16[2048,64]{0,1:T(8,128)(2,1)S(1)}, bf16[2048,64]{0,1:T(8,128)(2,1)}, u32[]{:S(2)}) copy-start(bf16[2048,64]{0,1:T(8,128)(2,1)} %param.19) | copy-start | bytes 786436
  0.0 8.4 %copy-start.13 = (bf16[2048,64]{0,1:T(8,128)(2,1)S(1)}, bf16[2048,64]{0,1:T(8,128)(2,1)}, u32[]{:S(2)}) copy-start(bf16[2048,64]{0,1:T(8,128)(2,1)} %param.20) | copy-start | bytes 786436
  0.8 8.7 %copy-start.14 = (bf16[2048,64]{0,1:T(8,128)(2,1)S(1)}, bf16[2048,64]{0,1:T(8,128)(2,1)}, u32[]{:S(2)}) copy-start(bf16[2048,64]{0,1:T(8,128)(2,1)} %param.21) | copy-start | bytes 786436
  0.8 9.7 %copy-start.15 = (bf16[2048,64]{0,1:T(8,128)(2,1)S(1)}, bf16[2048,64]{0,1:T(8,128)(2,1)}, u32[]{:S(2)}) copy-start(bf16[2048,64]{0,1:T(8,128)(2,1)} %param.22) | copy-start | bytes 786436
  27.2 2.7 %copy-start.18 = (bf16[1,64,64]{2,1,0:T(8,128)(2,1)S(1)}, bf16[1,64,64]{2,1,0:T(8,128)(2,1)}, u32[]{:S(2)}) copy-start(bf16[1,64,64]{2,1,0:T(8,128)(2,1)} %param.26) | copy-start | bytes 24580
  27.2 3.0 %copy-start.16 = (bf16[1,2048,64]{1,2,0:T(8,128)(2,1)S(1)}, bf16[1,2048,64]{1,2,0:T(8,128)(2,1)}, u32[]{:S(2)}) copy-start(bf16[1,2048,64]{1,2,0:T(8,128)(2,1)} %param.28) | copy-start | bytes 786436
  27.2 3.1 %copy-start.19 = (bf16[1,64,64]{2,1,0:T(8,128)(2,1)S(1)}, bf16[1,64,64]{2,1,0:T(8,128)(2,1)}, u32[]{:S(2)}) copy-start(bf16[1,64,64]{2,1,0:T(8,128)(2,1)} %param.29) | copy-start | bytes 24580
  27.2 12.8 %copy-start.17 = (s32[1,256,8]{1,2,0:T(8,128)S(1)}, s32[1,256,8]{1,2,0:T(8,128)}, u32[]{:S(2)}) copy-start(s32[1,256,8]{1,2,0:T(8,128)} %param.31) | copy-start | bytes 24580
  31.5 24.3 %all-to-all-start = ((bf16[16,1,64,128]{3,2,1,0:T(8,128)(2,1)}), bf16[16,1,64,128]{3,2,1,0:T(8,128)(2,1)}, u32[]{:S(2)}, u32[]{:S(2)}) async-start(bf16[16,1,64,128]{3,2,1,0:T(8,128)(2,1)} %broadcast_in_dim.34), calls=%async_computation | async-start | bytes 524288 | tf_op jit(solution)/shard_map/all_to_all | solution.py:20
  52.5 3.1 %copy-start.9 = (f32[2048,32]{0,1:T(8,128)S(1)}, f32[2048,32]{0,1:T(8,128)}, u32[]{:S(2)}) copy-start(f32[2048,32]{0,1:T(8,128)} %get-tuple-element.21) | copy-start | bytes 786436
  52.5 3.1 %copy-start.10 = (f32[2048,32]{0,1:T(8,128)S(1)}, f32[2048,32]{0,1:T(8,128)}, u32[]{:S(2)}) copy-start(f32[2048,32]{0,1:T(8,128)} %get-tuple-element.22) | copy-start | bytes 786436
  55.8 9.1 %copy-start.6 = (bf16[8,8,16,128]{3,1,2,0:T(8,128)(2,1)S(1)}, bf16[8,8,16,128]{3,1,2,0:T(8,128)(2,1)}, u32[]{:S(2)}) copy-start(bf16[8,8,16,128]{3,1,2,0:T(8,128)(2,1)} %get-tuple-element.11) | copy-start | bytes 786436
  55.8 67.7 %all-to-all-start.1 = ((bf16[1,16,16,64,128]{4,3,2,0,1:T(8,128)(2,1)}), bf16[1,16,16,64,128]{4,3,2,0,1:T(8,128)(2,1)}, u32[]{:S(2)}, u32[]{:S(2)}) async-start(bf16[1,16,16,64,128]{4,3,2,0,1:T(8,128)(2,1)} %bitcast.158), calls=%async_computation.1 | async-start | bytes 8388608 | tf_op jit(solution)/shard_map/all_to_all | solution.py:183
  72.6 10.6 %copy-start.20 = (f32[2048,2]{0,1:T(2,128)S(1)}, f32[2048,2]{0,1:T(2,128)}, u32[]{:S(2)}) copy-start(f32[2048,2]{0,1:T(2,128)} %get-tuple-element.7) | copy-start | bytes 49156
  127.9 5.8 %copy-start.7 = (bf16[2,4,16,8,128]{4,3,1,0,2:T(8,128)(2,1)S(1)}, bf16[2,4,16,8,128]{4,3,1,0,2:T(8,128)(2,1)}, u32[]{:S(2)}) copy-start(bf16[2,4,16,8,128]{4,3,1,0,2:T(8,128)(2,1)} %copy.104) | copy-start | bytes 786436
  130.8 2.9 %copy-start.8 = (bf16[2,4,16,8,128]{4,3,1,0,2:T(8,128)(2,1)S(1)}, bf16[2,4,16,8,128]{4,3,1,0,2:T(8,128)(2,1)}, u32[]{:S(2)}) copy-start(bf16[2,4,16,8,128]{4,3,1,0,2:T(8,128)(2,1)} %copy.103) | copy-start | bytes 786436
  132.2 1.6 copy-start.2
  135.3 7.2 %copy-start.3 = (bf16[1,16,640,128]{2,3,1,0:T(8,128)(2,1)S(1)}, bf16[1,16,640,128]{2,3,1,0:T(8,128)(2,1)}, u32[]{:S(2)}) copy-start(bf16[1,16,640,128]{2,3,1,0:T(8,128)(2,1)} %copy-done.2) | copy-start | bytes 7864324
  142.5 9.5 %copy-start.4 = (f32[16,8,8,256]{3,2,1,0:T(8,128)S(1)}, f32[16,8,8,256]{3,2,1,0:T(8,128)}, u32[]{:S(2)}) copy-start(f32[16,8,8,256]{3,2,1,0:T(8,128)} %copy.96) | copy-start | bytes 3145732
  152.1 17.6 %copy-start.23 = (bf16[1024,2048]{1,0:T(8,128)(2,1)S(1)}, bf16[1024,2048]{1,0:T(8,128)(2,1)}, u32[]{:S(2)}) copy-start(bf16[1024,2048]{1,0:T(8,128)(2,1)} %param.30) | copy-start | bytes 12582916
  152.1 19.8 %copy-start.1 = (bf16[1,2048,64]{1,2,0:T(8,128)(2,1)S(1)}, bf16[1,2048,64]{1,2,0:T(8,128)(2,1)}, u32[]{:S(2)}) copy-start(bf16[1,2048,64]{1,2,0:T(8,128)(2,1)} %param.25) | copy-start | bytes 786436
  (2 other events, 2.8 us)
where the time goes:
time: 173 us; the launch traced here: 172 us
  local copies, waits for them, and re-layouts  44 us (25%)
  matrix products  39.3 us (23%)
  waiting for transfers between devices  29.5 us (17%)
  other arithmetic  27.4 us (16%)
  blocking collectives  15.9 us (9%)
  starting transfers between devices  15.3 us (9%)
    all_to_all x1, waiting for transfers between devices, per_device(): lax.all_to_all(outgoing, 'kv', split_axis=1, concat_axis=1, tiled=True)  29.5 us
    all_to_all x1, blocking collectives, per_device(): lax.all_to_all(mixed, 'tp', split_axis=0, concat_axis=1, tiled=True)  15.9 us
    sub x1, matrix products, per_device(): jax.nn.softmax(jnp.where(usable, cmp_scores, masked_score), axis=-1)  10.6 us
    unnamed x58, local copies, waits for them, and re-layouts  10.2 us
    dot_general x1, matrix products, per_device(): jnp.einsum('ktgc,kcd->ktgd', cmp_probs.astype(jnp.bfloat16), summaries[.....  9.4 us
    dot_general x1, matrix products, per_device(): jnp.dot(normed, joined_weight, preferred_element_type=jnp.float32)  9.36 us
    all_to_all x1, starting transfers between devices, copy_for_each(): lax.all_to_all(jnp.broadcast_to(x[None], (peers, *x.shape)), axis, 0, 0,...  8.48 us
    sub x1, other arithmetic, per_device(): jax.nn.softmax(jnp.where(allowed_keys, sel_scores, masked_score), axis=-1)  7.17 us
  transfers between devices with their start and end apart: 2, of which 1 were waited for; matrix products, arithmetic and copies ran while one was open for 27% of the time, Pallas kernels for 0%

commit v1 on v0

v1 whole, which is shorter than its diff:
```python
import functools

import jax
import jax.numpy as jnp
import numpy as np
from jax import lax
from jax.experimental import pallas as pl
from jax.experimental.pallas import tpu as pltpu
from jax.sharding import PartitionSpec as P

HEAD_DIM = 64
CMP_BLOCK = 32
SEL_BLOCK = 64
Q_BLOCK = 128
FAR_PICKS = 8
ROPE_BASE = 10000.0
NORM_EPS = 1e-06
MASKED = -1e30
LANES = 128
TILE = 256

F32 = jnp.float32
BF16 = jnp.bfloat16


def dot_nt(a, b):
    return lax.dot_general(a, b, (((1,), (1,)), ((), ())), preferred_element_type=F32)


def rope_tables(total):
    lane = np.arange(LANES)
    inverse = ROPE_BASE ** (-(lane % 32) / 32.0)
    sign = np.where(lane % 64 < 32, -1.0, 1.0)
    coarse = (np.arange(total // TILE) * TILE)[:, None] * inverse[None, :]
    fine = np.arange(TILE)[:, None] * inverse[None, :]
    pack = lambda a: np.stack([np.cos(a), np.sin(a) * sign[None, :]], axis=1).astype(np.float32)
    return pack(coarse), pack(fine).transpose(1, 0, 2)


def project_kernel(
    meta, tok_ref, gain_ref, wq_ref, sk_ref, sv_ref, ck_ref, cv_ref, bw_ref, coarse_ref, fine_ref,
    ke_ref, ki_ref, ko_ref, ve_ref, vi_ref, vo_ref,
    qp_ref, qt_ref, kv_ref, gc_ref, gs_ref, first_ref, second_ref,
    w_scr, kv_scr, c_scr,
):
    step = pl.program_id(0)
    lane = lax.broadcasted_iota(jnp.int32, (TILE, LANES), 1)
    low = lane < HEAD_DIM

    @pl.when(step == 0)
    def _():
        w_scr[:, 0:LANES] = wq_ref[...]
        w_scr[:, LANES:2 * LANES] = jnp.concatenate([sk_ref[...], sv_ref[...]], axis=0).T
        w_scr[:, 2 * LANES:3 * LANES] = jnp.concatenate([ck_ref[...], cv_ref[...]], axis=0).T
        bw = bw_ref[...]
        pad = jnp.zeros((LANES - bw.shape[0], bw.shape[1]), BF16)
        w_scr[:, 3 * LANES:4 * LANES] = jnp.concatenate([bw, pad], axis=0).T

    x = tok_ref[...].astype(F32)
    mean = jnp.mean(x * x, axis=-1, keepdims=True)
    normed = (x * lax.rsqrt(mean + NORM_EPS) * gain_ref[...].astype(F32)).astype(BF16)
    proj = jnp.dot(normed, w_scr[...], preferred_element_type=F32)

    ch = coarse_ref[0, 0:1, :]
    sh = coarse_ref[0, 1:2, :]
    cl = fine_ref[0]
    sl = fine_ref[1]
    cosine = ch * cl - sh * sl
    sine = sh * cl + ch * sl
    first_half = (lane % HEAD_DIM) < 32

    def turn(v):
        swapped = jnp.where(first_half, pltpu.roll(v, LANES - 32, 1), pltpu.roll(v, 32, 1))
        return v * cosine + swapped * sine

    q = proj[:, 0:LANES]
    scale = HEAD_DIM ** (-0.5)
    plain = q * scale
    turned = turn(q) * scale
    qp_ref[0] = jnp.where(low, plain, 0.0).astype(BF16)
    qp_ref[1] = jnp.where(low, pltpu.roll(plain, HEAD_DIM, 1), 0.0).astype(BF16)
    qt_ref[0] = jnp.where(low, turned, 0.0).astype(BF16)
    qt_ref[1] = jnp.where(low, pltpu.roll(turned, HEAD_DIM, 1), 0.0).astype(BF16)
    kv = proj[:, LANES:2 * LANES]
    kv = jnp.where(low, turn(kv), kv).astype(BF16)
    kv_ref[...] = kv
    per = TILE // SEL_BLOCK
    kv_scr[pl.ds(step * per, per)] = kv.reshape(per, SEL_BLOCK, LANES)
    rows = pl.multiple_of(step * TILE, TILE)
    c_scr[pl.ds(rows, TILE), :] = proj[:, 2 * LANES:3 * LANES].astype(BF16).astype(F32)
    heads = meta[meta.shape[0] - 1] * 2
    logits = pltpu.roll(proj[:, 3 * LANES:4 * LANES], LANES - heads, 1)
    gates = 1.0 / (1.0 + jnp.exp(-logits))
    gc_ref[...] = jnp.where(low, gates[:, 0:1], gates[:, 1:2])
    gs_ref[...] = jnp.where(low, gates[:, 16:17], gates[:, 17:18])

    @pl.when(step == pl.num_programs(0) - 1)
    def _():
        blocks = first_ref.shape[2]
        low_b = lax.broadcasted_iota(jnp.int32, (blocks, LANES), 1) < HEAD_DIM
        key_parts = []
        value_parts = []
        for pair in range(CMP_BLOCK // 2):
            two = []
            for r in (2 * pair, 2 * pair + 1):
                embed = jnp.concatenate([ke_ref[r:r + 1, :], ve_ref[r:r + 1, :]], axis=1).astype(F32)
                two.append(c_scr[pl.ds(r, blocks, stride=CMP_BLOCK), :] + embed)
            a, b = two
            key_parts.append(jnp.where(low_b, a, pltpu.roll(b, HEAD_DIM, 1)).astype(BF16))
            value_parts.append(jnp.where(low_b, pltpu.roll(a, HEAD_DIM, 1), b).astype(BF16))
        hidden_k = jax.nn.gelu(dot_nt(jnp.concatenate(key_parts, axis=1), ki_ref[...])).astype(BF16)
        hidden_v = jax.nn.gelu(dot_nt(jnp.concatenate(value_parts, axis=1), vi_ref[...])).astype(BF16)
        summary = jnp.concatenate(
            [
                jnp.dot(hidden_k, ko_ref[...], preferred_element_type=F32),
                jnp.dot(hidden_v, vo_ref[...], preferred_element_type=F32),
            ],
            axis=1,
        ).astype(BF16)
        owners = first_ref.shape[0]
        half = second_ref.shape[1]

        def fill(d, carry):
            for j in range(half):
                first_ref[d, j] = kv_scr[meta[d * 2 * half + 2 * j]]
                second_ref[d, j] = kv_scr[meta[d * 2 * half + 2 * j + 1]]
            first_ref[d, half] = summary
            return carry

        lax.fori_loop(0, owners, fill, 0)


def compress_kernel(meta, qp_ref, sum_ref, gc_ref, out_ref, v_scr):
    step = pl.program_id(0)
    owners, _, blocks, _ = sum_ref.shape
    count = owners * blocks

    @pl.when(step == 0)
    def _():
        low_k = lax.broadcasted_iota(jnp.int32, (count, LANES), 1) < HEAD_DIM
        v_scr[...] = jnp.where(low_k, 1.0, sum_ref[...].reshape(count, LANES).astype(F32)).astype(BF16)

    keys = sum_ref[...].reshape(count, LANES)
    q = qp_ref[...].reshape(2 * Q_BLOCK, LANES)
    scores = dot_nt(q, keys)
    base = meta[0] + step * Q_BLOCK
    row = lax.broadcasted_iota(jnp.int32, (2 * Q_BLOCK, 1), 0) % Q_BLOCK
    limit = (base + row + 1) // CMP_BLOCK
    col = lax.broadcasted_iota(jnp.int32, (2 * Q_BLOCK, count), 1)
    scores = jnp.where(col < limit, scores, MASKED)
    top = jnp.max(scores, axis=-1, keepdims=True)
    probs = jnp.exp(scores - top).astype(BF16)
    mixed = jnp.dot(probs, v_scr[...], preferred_element_type=F32)
    total = pltpu.roll(mixed, HEAD_DIM, 1)
    out = jnp.where(limit > 0, mixed / total, 0.0)
    low = lax.broadcasted_iota(jnp.int32, (Q_BLOCK, LANES), 1) < HEAD_DIM
    joined = jnp.where(low, pltpu.roll(out[:Q_BLOCK], HEAD_DIM, 1), out[Q_BLOCK:])
    out_ref[...] = gc_ref[...] * joined


def select_kernel(src, qt_ref, kv_ref, in_ref, bias_ref, gs_ref, cmp_ref, out_ref, k_scr, v_scr, *, parity):
    step = pl.program_id(0)
    k_scr[0:Q_BLOCK, :] = kv_ref[...]
    block = 2 * step + parity
    for j in range(FAR_PICKS):
        k_scr[Q_BLOCK + j * SEL_BLOCK:Q_BLOCK + (j + 1) * SEL_BLOCK, :] = in_ref[src[block * FAR_PICKS + j], 0]
    keys = k_scr[...]
    total_keys = keys.shape[0]
    low_k = lax.broadcasted_iota(jnp.int32, (total_keys, LANES), 1) < HEAD_DIM
    v_scr[...] = jnp.where(low_k, 1.0, keys.astype(F32)).astype(BF16)
    q = qt_ref[...].reshape(2 * Q_BLOCK, LANES)
    scores = dot_nt(q, keys)
    row = lax.broadcasted_iota(jnp.int32, (2 * Q_BLOCK, Q_BLOCK), 0) % Q_BLOCK
    col = lax.broadcasted_iota(jnp.int32, (2 * Q_BLOCK, Q_BLOCK), 1)
    own = jnp.where(col <= row, scores[:, :Q_BLOCK], MASKED)
    far = scores[:, Q_BLOCK:] + bias_ref[0]
    top = jnp.maximum(jnp.max(own, axis=-1, keepdims=True), jnp.max(far, axis=-1, keepdims=True))
    probs_own = jnp.exp(own - top).astype(BF16)
    probs_far = jnp.exp(far - top).astype(BF16)
    mixed = jnp.dot(jnp.concatenate([probs_own, probs_far], axis=1), v_scr[...], preferred_element_type=F32)
    out = mixed / pltpu.roll(mixed, HEAD_DIM, 1)
    low = lax.broadcasted_iota(jnp.int32, (Q_BLOCK, LANES), 1) < HEAD_DIM
    joined = jnp.where(low, pltpu.roll(out[:Q_BLOCK], HEAD_DIM, 1), out[Q_BLOCK:])
    out_ref[0] = (cmp_ref[...] + gs_ref[...] * joined).astype(BF16)


def whole(shape):
    return pl.BlockSpec(shape, lambda i, *_: (0,) * len(shape))


def per_device(
    tokens, norm_gain, query_weight, cmp_key_weight, cmp_value_weight, sel_key_weight, sel_value_weight,
    branch_weight, key_embed, key_inner, key_outer, value_embed, value_inner, value_outer, out_weight, chosen,
):
    tok_rows, width = tokens.shape
    owners = lax.axis_size("kv")
    dev = lax.axis_index("kv")
    tp = lax.axis_index("tp")
    span_queries = tok_rows // Q_BLOCK
    span_blocks = tok_rows // SEL_BLOCK
    cmp_blocks = tok_rows // CMP_BLOCK
    half = span_queries // 2
    picks = chosen[0]
    match = picks // span_blocks == dev
    wanted = jnp.sum(jnp.where(match, picks % span_blocks, 0), axis=1).astype(jnp.int32)
    meta = jnp.concatenate([wanted, jnp.stack([dev, tp]).astype(jnp.int32)])
    my_picks = lax.dynamic_slice_in_dim(picks, dev * span_queries, span_queries, 0)
    source = (my_picks // span_blocks).astype(jnp.int32).reshape(-1)
    own_block = (dev * span_queries + jnp.arange(span_queries, dtype=jnp.int32)) * (Q_BLOCK // SEL_BLOCK)
    bias = jnp.where(my_picks < own_block[:, None], 0.0, MASKED).astype(F32)
    bias = jnp.repeat(bias, SEL_BLOCK, axis=1)[:, None, :]

    coarse, fine = rope_tables(owners * tok_rows)
    steps = tok_rows // TILE
    n_meta = meta.shape[0]
    gates_t = branch_weight.transpose(0, 2, 1).reshape(-1, width)
    tile = lambda: pl.BlockSpec((TILE, LANES), lambda i, m: (i, 0))
    heads_tile = lambda: pl.BlockSpec((2, TILE, LANES), lambda i, m: (0, i, 0))
    slots = lambda n: jax.ShapeDtypeStruct((owners, n, SEL_BLOCK, LANES), BF16)
    qp, qt, kv, gate_cmp, gate_sel, first, second = pl.pallas_call(
        project_kernel,
        grid_spec=pltpu.PrefetchScalarGridSpec(
            num_scalar_prefetch=1,
            grid=(steps,),
            in_specs=[
                pl.BlockSpec((TILE, width), lambda i, m: (i, 0)),
                whole((1, width)),
                whole((width, LANES)),
                whole((HEAD_DIM, width)),
                whole((HEAD_DIM, width)),
                whole((HEAD_DIM, width)),
                whole((HEAD_DIM, width)),
                whole(gates_t.shape),
                pl.BlockSpec((1, 2, LANES), lambda i, m: (m[n_meta - 2] * steps + i, 0, 0)),
                whole((2, TILE, LANES)),
                whole((CMP_BLOCK, HEAD_DIM)),
                whole((HEAD_DIM, CMP_BLOCK * HEAD_DIM)),
                whole((HEAD_DIM, HEAD_DIM)),
                whole((CMP_BLOCK, HEAD_DIM)),
                whole((HEAD_DIM, CMP_BLOCK * HEAD_DIM)),
                whole((HEAD_DIM, HEAD_DIM)),
            ],
            out_specs=[
                heads_tile(), heads_tile(), tile(), tile(), tile(),
                whole((owners, half + 1, SEL_BLOCK, LANES)),
                whole((owners, half, SEL_BLOCK, LANES)),
            ],
            scratch_shapes=[
                pltpu.VMEM((width, 4 * LANES), BF16),
                pltpu.VMEM((span_blocks, SEL_BLOCK, LANES), BF16),
                pltpu.VMEM((tok_rows, LANES), F32),
            ],
        ),
        out_shape=[
            jax.ShapeDtypeStruct((2, tok_rows, LANES), BF16),
            jax.ShapeDtypeStruct((2, tok_rows, LANES), BF16),
            jax.ShapeDtypeStruct((tok_rows, LANES), BF16),
            jax.ShapeDtypeStruct((tok_rows, LANES), F32),
            jax.ShapeDtypeStruct((tok_rows, LANES), F32),
            slots(half + 1),
            slots(half),
        ],
        compiler_params=pltpu.CompilerParams(
            dimension_semantics=("arbitrary",), vmem_limit_bytes=48 * 1024 * 1024
        ),
        name="project",
    )(
        meta, tokens, norm_gain.reshape(1, width), query_weight, sel_key_weight.T, sel_value_weight.T,
        cmp_key_weight.T, cmp_value_weight.T, gates_t, jnp.asarray(coarse), jnp.asarray(fine),
        key_embed[0], key_inner[0].T, key_outer[0], value_embed[0], value_inner[0].T, value_outer[0],
    )
    first = lax.all_to_all(first, "kv", 0, 0, tiled=True)
    second = lax.all_to_all(second, "kv", 0, 0, tiled=True)

    base = (dev * tok_rows).astype(jnp.int32).reshape(1)
    gated = pl.pallas_call(
        compress_kernel,
        grid_spec=pltpu.PrefetchScalarGridSpec(
            num_scalar_prefetch=1,
            grid=(span_queries,),
            in_specs=[
                pl.BlockSpec((2, Q_BLOCK, LANES), lambda i, m: (0, i, 0)),
                pl.BlockSpec((owners, 1, cmp_blocks, LANES), lambda i, m: (0, half, 0, 0)),
                pl.BlockSpec((Q_BLOCK, LANES), lambda i, m: (i, 0)),
            ],
            out_specs=pl.BlockSpec((Q_BLOCK, LANES), lambda i, m: (i, 0)),
            scratch_shapes=[pltpu.VMEM((owners * cmp_blocks, LANES), BF16)],
        ),
        out_shape=jax.ShapeDtypeStruct((tok_rows, LANES), F32),
        compiler_params=pltpu.CompilerParams(
            dimension_semantics=("arbitrary",), vmem_limit_bytes=48 * 1024 * 1024
        ),
        name="compress",
    )(base, qp, first, gate_cmp)

    def select(incoming, parity):
        return pl.pallas_call(
            functools.partial(select_kernel, parity=parity),
            grid_spec=pltpu.PrefetchScalarGridSpec(
                num_scalar_prefetch=1,
                grid=(half,),
                in_specs=[
                    pl.BlockSpec((2, Q_BLOCK, LANES), lambda i, m: (0, 2 * i + parity, 0)),
                    pl.BlockSpec((Q_BLOCK, LANES), lambda i, m: (2 * i + parity, 0)),
                    pl.BlockSpec((owners, 1, SEL_BLOCK, LANES), lambda i, m: (0, i, 0, 0)),
                    pl.BlockSpec((1, 1, FAR_PICKS * SEL_BLOCK), lambda i, m: (2 * i + parity, 0, 0)),
                    pl.BlockSpec((Q_BLOCK, LANES), lambda i, m: (2 * i + parity, 0)),
                    pl.BlockSpec((Q_BLOCK, LANES), lambda i, m: (2 * i + parity, 0)),
                ],
                out_specs=pl.BlockSpec((1, Q_BLOCK, LANES), lambda i, m: (i, 0, 0)),
                scratch_shapes=[
                    pltpu.VMEM((Q_BLOCK + FAR_PICKS * SEL_BLOCK, LANES), BF16),
                    pltpu.VMEM((Q_BLOCK + FAR_PICKS * SEL_BLOCK, LANES), BF16),
                ],
            ),
            out_shape=jax.ShapeDtypeStruct((half, Q_BLOCK, LANES), BF16),
            compiler_params=pltpu.CompilerParams(
                dimension_semantics=("arbitrary",), vmem_limit_bytes=48 * 1024 * 1024
            ),
            name="select",
        )(source, qt, kv, incoming, bias, gate_sel, gated)

    outs = []
    for incoming, parity in ((first, 0), (second, 1)):
        mixed = select(incoming, parity)
        rows = lax.all_to_all(mixed, "tp", 0, 0, tiled=True)
        weight = out_weight.reshape(rows.shape[0], LANES, out_weight.shape[1])
        outs.append(jnp.einsum("trc,tcd->rd", rows, weight, preferred_element_type=F32).astype(BF16))
    return jnp.concatenate(outs, axis=0)


def solution(mesh):
    placed = (
        P("kv", None),
        P(),
        P(None, "tp"),
        P(None, "tp"),
        P(None, "tp"),
        P(None, "tp"),
        P(None, "tp"),
        P(),
        P("tp", None, None),
        P("tp", None, None),
        P("tp", None, None),
        P("tp", None, None),
        P("tp", None, None),
        P("tp", None, None),
        P(),
        P("tp", None, None),
    )
    return jax.shard_map(
        per_device, mesh=mesh, in_specs=placed, out_specs=P(("kv", "tp"), None), check_vma=False
    )
```

time: 173 us -> 142 us (0.82)
  Pallas kernels: 0 us -> 46.8 us
  matrix products: 39.3 us -> 5.9 us
  waiting for transfers between devices: 29.5 us -> 3.98 us
  other arithmetic: 27.4 us -> 1.98 us
  blocking collectives: 15.9 us -> 38.9 us
  local copies, waits for them, and re-layouts: 44 us -> 25.7 us
  starting transfers between devices: 15.3 us -> 17.3 us
    pallas_call x0 -> x4, Pallas kernels: none -> 46.8 us  [the longest x2 17.4 us: select(): pl.pallas_call(functools.partial(select_kernel, parity=parity), grid_spec...]
    all_to_all x2 -> x3, waiting for transfers between devices: 29.5 us -> 3.98 us  [the longest x2 3.47 us: per_device(): rows = lax.all_to_all(mixed, 'tp', 0, 0, tiled=True)]
    all_to_all x1, blocking collectives: 15.9 us -> 38.9 us  [per_device(): first = lax.all_to_all(first, 'kv', 0, 0, tiled=True)]
    dot_general x7 -> x2, matrix products: 28.7 us -> 5.9 us  [per_device(): jnp.einsum('trc,tcd->rd', rows, weight, preferred_element_type=F32)]
    unnamed x58 -> x54, local copies, waits for them, and re-layouts: 10.2 us -> 24.6 us
    sub x1 -> x0, matrix products: 10.6 us -> none  [per_device(): jax.nn.softmax(jnp.where(usable, cmp_scores, masked_score), axis=-1)]
    concatenate x13 -> x0, local copies, waits for them, and re-layouts: 9.58 us -> none  [the longest x1 5.46 us: per_device(): jnp.concatenate([query_weight, cmp_key_weight, cmp_value_weight, sel_key_...]
    gather x2 -> x0, local copies, waits for them, and re-layouts: 7.53 us -> none  [the longest x1 4.46 us: per_device(): picked = incoming[head_lane, source, query_lane]]
  transfers between devices with their start and end apart: 2 -> 3, of which waited for: 1 -> 2; matrix products, arithmetic and copies ran while one was open for 27% -> 2% of each run, Pallas kernels for 0% -> 21%
where the time goes in v1:
time: 142 us; the launch traced here: 141 us
  Pallas kernels  46.8 us (33%)
  blocking collectives  38.9 us (27%)
  local copies, waits for them, and re-layouts  25.7 us (18%)
  starting transfers between devices  17.3 us (12%)
  matrix products  5.9 us (4%)
  waiting for transfers between devices  3.98 us (3%)
  other arithmetic  1.98 us (1%)
    all_to_all x1, blocking collectives, per_device(): first = lax.all_to_all(first, 'kv', 0, 0, tiled=True)  38.9 us
    unnamed x54, local copies, waits for them, and re-layouts  24.6 us
    pallas_call x2, Pallas kernels, select(): pl.pallas_call(functools.partial(select_kernel, parity=parity), grid_spec...  17.4 us
    pallas_call x1, Pallas kernels, per_device(): pl.pallas_call(project_kernel, grid_spec=pltpu.PrefetchScalarGridSpec(num...  16.9 us
    all_to_all x2, starting transfers between devices, per_device(): rows = lax.all_to_all(mixed, 'tp', 0, 0, tiled=True)  12.8 us
    pallas_call x1, Pallas kernels, per_device(): pl.pallas_call(compress_kernel, grid_spec=pltpu.PrefetchScalarGridSpec(nu...  12.5 us
    dot_general x2, matrix products, per_device(): jnp.einsum('trc,tcd->rd', rows, weight, preferred_element_type=F32)  5.9 us
    all_to_all x1, starting transfers between devices, per_device(): second = lax.all_to_all(second, 'kv', 0, 0, tiled=True)  4.44 us
  transfers between devices with their start and end apart: 3, of which 2 were waited for; matrix products, arithmetic and copies ran while one was open for 2% of the time, Pallas kernels for 21%

profile of v1, /device:TPU:1, one launch (start us, length us, event | category | flops | bytes accessed | tf_op | source)
XLA Modules:
  0.0 140.6 jit_solution(7049378087925046026)
XLA Ops:
  1.5 1.0 copy-done.12
  2.5 0.9 copy-done.13
  13.8 16.9 %project.1 = (bf16[2,2048,128]{2,1,0:T(8,128)(2,1)S(1)}, bf16[2,2048,128]{2,1,0:T(8,128)(2,1)S(1)}, bf16[2048,128]{1,0:T(8,128)(2,1)S(1)}, f32[2048,128]{1,0:T(8...) custom-call(s32[258]{0:T(512)S(1)} %pad_add_fusion.meta, ...), custom_call_target="tpu_custom_call" | custom-call | tf_op jit(solution)/shard_map/project/pallas_call | solution.py:220
  30.8 1.0 copy-done.1
  32.6 1.0 copy-done.9
  33.6 38.9 %all_to_all.20.sum_ref.in_ref = bf16[16,9,64,128]{3,2,1,0:T(8,128)(2,1)S(1)} all-to-all(bf16[16,9,64,128]{3,2,1,0:T(8,128)(2,1)} %get-tuple-element.14), channel_id=1, replica_groups=mesh['kv'=16,'tp'=8] {'kv'}, dimensions={0} | all-to-all | bytes 4718592 | tf_op jit(solution)/shard_map/all_to_all | solution.py:272
  72.5 4.4 %all-to-all-start.2 = ((bf16[16,8,64,128]{3,2,1,0:T(8,128)(2,1)}), bf16[16,8,64,128]{3,2,1,0:T(8,128)(2,1)}, u32[]{:S(2)}, u32[]{:S(2)}) async-start(bf16[16,8,64,128]{3,2,1,0:T(8,128)(2,1)} %get-tuple-element.18), calls=%async_computation.2 | async-start | bytes 4194304 | tf_op jit(solution)/shard_map/all_to_all | solution.py:273
  77.5 1.2 copy-done.10
  78.7 1.2 copy-done.11
  80.0 12.5 %compress.1.cmp_ref = f32[2048,128]{1,0:T(8,128)S(1)} custom-call(s32[1]{0:T(128)} %bitcast.18.meta, bf16[2,2048,128]{2,1,0:T(8,128)(2,1)S(1)} %copy-done.10, bf16[16,9,64,128]{3,2,1,0:T(8,128)(2,1)S(1)} %all_to_all.20.sum_ref.in_ref, f32[2048,128]{1,0:T(8,128)S(1)} %copy-done.11), custom_call_target="tpu_custom_call" | custom-call | tf_op jit(solution)/shard_map/compress/pallas_call | solution.py:276
  92.5 1.2 copy-done.2
  93.7 1.2 copy-done.4
  94.9 1.0 copy-done.7
  95.9 8.7 %select.16 = bf16[8,128,128]{2,1,0:T(8,128)(2,1)} custom-call(s32[128]{0:T(128)S(1)} %and_select_fusion.src, bf16[2,2048,128]{2,1,0:T(8,128)(2,1)S(1)} %copy-done.2, bf16[2048,128]{1,0:T(8,128)(2,1)S(1)} %copy-done.7, bf16[16,9,64,128]{3,2,1,0:T(8,128)(2,1)} %copy-done, f32[16,1,512]{2,1,0:T(1,128)S(1)} %broadcast_in_dim_reshape.3.bias_ref, ...), custom_call_target="tpu_custom_call" | custom-call | tf_op jit(solution)/shard_map/select/pallas_call | solution.py:297
  105.1 8.0 %all-to-all-start.1 = ((bf16[8,128,128]{2,1,0:T(8,128)(2,1)}), bf16[8,128,128]{2,1,0:T(8,128)(2,1)}, u32[]{:S(2)}, u32[]{:S(2)}) async-start(bf16[8,128,128]{2,1,0:T(8,128)(2,1)} %select.16), calls=%async_computation.1 | async-start | bytes 524288 | tf_op jit(solution)/shard_map/all_to_all | solution.py:326
  113.2 1.2 copy-done.3
  114.4 1.2 copy-done.5
  115.6 1.0 copy-done.8
  116.7 8.7 %select.17 = bf16[8,128,128]{2,1,0:T(8,128)(2,1)} custom-call(s32[128]{0:T(128)S(1)} %and_select_fusion.src, bf16[2,2048,128]{2,1,0:T(8,128)(2,1)S(1)} %copy-done.3, bf16[2048,128]{1,0:T(8,128)(2,1)S(1)} %copy-done.8, bf16[16,8,64,128]{3,2,1,0:T(8,128)(2,1)} %all-to-all-done.2.in_ref, f32[16,1,512]{2,1,0:T(1,128)S(1)} %broadcast_in_dim_reshape.3.bias_ref, ...), custom_call_target="tpu_custom_call" | custom-call | tf_op jit(solution)/shard_map/select/pallas_call | solution.py:297
  125.4 4.8 %all-to-all-start.3 = ((bf16[8,128,128]{2,1,0:T(8,128)(2,1)}), bf16[8,128,128]{2,1,0:T(8,128)(2,1)S(1)}, u32[]{:S(2)}, u32[]{:S(2)}) async-start(bf16[8,128,128]{2,1,0:T(8,128)(2,1)} %select.17), calls=%async_computation.3 | async-start | bytes 524288 | tf_op jit(solution)/shard_map/all_to_all | solution.py:326
  130.2 3.0 %fusion = bf16[128,2048]{1,0:T(8,128)(2,1)S(1)} fusion(bf16[8,128,128]{2,1,0:T(8,128)(2,1)} %all-to-all-done.1, bf16[8,128,2048]{2,1,0:T(8,128)(2,1)} %bitcast.66), kind=kOutput, calls=%fused_computation.2 | convolution fusion | flops 537133056 | bytes 4980736 | tf_op jit(solution)/shard_map/trc,tcd->rd/dot_general | solution.py:328
  133.2 3.5 %all-to-all-done.3 = bf16[8,128,128]{2,1,0:T(8,128)(2,1)S(1)} async-done(((bf16[8,128,128]{2,1,0:T(8,128)(2,1)}), bf16[8,128,128]{2,1,0:T(8,128)(2,1)S(1)}, u32[]{:S(2)}, u32[]{:S(2)}) %all-to-all-start.3) | async-done | bytes 262176 | tf_op jit(solution)/shard_map/all_to_all | solution.py:326
  136.7 2.9 %fusion.1 = bf16[128,2048]{1,0:T(8,128)(2,1)S(1)} fusion(bf16[8,128,128]{2,1,0:T(8,128)(2,1)S(1)} %all-to-all-done.3, bf16[8,128,2048]{2,1,0:T(8,128)(2,1)} %bitcast.67), kind=kOutput, calls=%fused_computation.3 | convolution fusion | flops 537133056 | bytes 4980736 | tf_op jit(solution)/shard_map/trc,tcd->rd/dot_general | solution.py:328
  139.6 1.1 pad_maximum_fusion
  (55 shorter events, 13.7 us)
Async XLA Ops:
  1.5 1.0 copy-start.12
  2.5 0.9 copy-start.13
  3.5 0.9 copy-start.14
  4.4 0.9 copy-start.15
  5.4 0.9 copy-start.16
  6.3 0.9 copy-start.17
  7.3 0.9 copy-start.18
  8.2 0.9 copy-start.19
  9.2 0.9 copy-start.20
  30.7 1.0 copy-start.1
  32.6 1.0 copy-start.9
  33.6 43.4 %copy-start.26 = (s32[1,256,8]{1,2,0:T(8,128)S(1)}, s32[1,256,8]{1,2,0:T(8,128)}, u32[]{:S(2)}) copy-start(s32[1,256,8]{1,2,0:T(8,128)} %param.33) | copy-start | bytes 24580
  72.5 19.9 %copy-start = (bf16[16,9,64,128]{3,2,1,0:T(8,128)(2,1)}, bf16[16,9,64,128]{3,2,1,0:T(8,128)(2,1)S(1)}, u32[]{:S(2)}) copy-start(bf16[16,9,64,128]{3,2,1,0:T(8,128)(2,1)S(1)} %all_to_all.20.sum_ref.in_ref) | copy-start | bytes 7077892
  72.5 32.6 %all-to-all-start.2 = ((bf16[16,8,64,128]{3,2,1,0:T(8,128)(2,1)}), bf16[16,8,64,128]{3,2,1,0:T(8,128)(2,1)}, u32[]{:S(2)}, u32[]{:S(2)}) async-start(bf16[16,8,64,128]{3,2,1,0:T(8,128)(2,1)} %get-tuple-element.18), calls=%async_computation.2 | async-start | bytes 4194304 | tf_op jit(solution)/shard_map/all_to_all | solution.py:273
  77.5 1.2 copy-start.10
  78.7 1.2 copy-start.11
  92.4 1.2 copy-start.2
  93.7 1.2 copy-start.4
  94.9 1.0 copy-start.7
  105.1 20.2 %all-to-all-start.1 = ((bf16[8,128,128]{2,1,0:T(8,128)(2,1)}), bf16[8,128,128]{2,1,0:T(8,128)(2,1)}, u32[]{:S(2)}, u32[]{:S(2)}) async-start(bf16[8,128,128]{2,1,0:T(8,128)(2,1)} %select.16), calls=%async_computation.1 | async-start | bytes 524288 | tf_op jit(solution)/shard_map/all_to_all | solution.py:326
  113.2 1.2 copy-start.3
  114.4 1.2 copy-start.5
  115.6 1.0 copy-start.8
  125.4 11.3 %all-to-all-start.3 = ((bf16[8,128,128]{2,1,0:T(8,128)(2,1)}), bf16[8,128,128]{2,1,0:T(8,128)(2,1)S(1)}, u32[]{:S(2)}, u32[]{:S(2)}) async-start(bf16[8,128,128]{2,1,0:T(8,128)(2,1)} %select.17), calls=%async_computation.3 | async-start | bytes 524288 | tf_op jit(solution)/shard_map/all_to_all | solution.py:326
  (6 other events, 4.6 us)

commit v2 on v1

v2 whole, which is shorter than its diff:
```python
import functools

import jax
import jax.numpy as jnp
import numpy as np
from jax import lax
from jax.experimental import pallas as pl
from jax.experimental.pallas import tpu as pltpu
from jax.sharding import PartitionSpec as P

HEAD_DIM = 64
CMP_BLOCK = 32
SEL_BLOCK = 64
Q_BLOCK = 128
FAR_PICKS = 8
ROPE_BASE = 10000.0
NORM_EPS = 1e-06
MASKED = -1e30
LANES = 128
TILE = 256
SPAN_BLOCKS = 32
LOG2E = 1.4426950408889634
TOGETHER = 4

F32 = jnp.float32
BF16 = jnp.bfloat16


def dot_nt(a, b):
    return lax.dot_general(a, b, (((1,), (1,)), ((), ())), preferred_element_type=F32)


def rope_tables(total):
    lane = np.arange(LANES)
    inverse = ROPE_BASE ** (-(lane % 32) / 32.0)
    sign = np.where(lane % 64 < 32, -1.0, 1.0)
    coarse = (np.arange(total // TILE) * TILE)[:, None] * inverse[None, :]
    fine = np.arange(TILE)[:, None] * inverse[None, :]
    pack = lambda a: np.stack([np.cos(a), np.sin(a) * sign[None, :]], axis=1).astype(np.float32)
    return pack(coarse), pack(fine).transpose(1, 0, 2)


def wanted_blocks(picks, dev, span_blocks):
    match = picks // span_blocks == dev
    return jnp.sum(jnp.where(match, picks % span_blocks, 0), axis=0, keepdims=True)


def project_kernel(dev_ref, tp_ref, *refs):
    n_in = 17
    tok_ref, *rest = refs[:n_in]
    coarse_ref = rest.pop(9)
    qp_ref, qt_ref, kv_ref, gc_ref, gs_ref, first_ref = refs[n_in:n_in + 6]
    tok_scr, *local = refs[n_in + 6:2 * n_in + 6]
    coarse_scr = local.pop(9)
    (
        gain_scr, wq_scr, sk_scr, sv_scr, ck_scr, cv_scr, bw_scr, pick_scr, fine_scr,
        ke_scr, ki_scr, ko_scr, ve_scr, vi_scr, vo_scr,
    ) = local
    (
        qp_scr, qt_scr, kv_scr, gc_scr, gs_scr, first_scr, w_scr, raw_scr, inv_scr, c_scr, xk_scr, xv_scr,
        want_vmem, want_smem, tok_sem, in_sem, want_sem, out_sem,
    ) = refs[2 * n_in + 6:]
    tiles = tok_scr.shape[0]
    owners, slots = first_scr.shape[:2]
    half = slots - 1
    span_blocks = kv_scr.shape[0]
    lane = lax.broadcasted_iota(jnp.int32, (TILE, LANES), 1)
    low = lane < HEAD_DIM

    def tile_copy(t):
        return pltpu.make_async_copy(tok_ref.at[pl.ds(t * TILE, TILE), :], tok_scr.at[t], tok_sem.at[t])

    copies = [pltpu.make_async_copy(src, dst, in_sem.at[i]) for i, (src, dst) in enumerate(zip(rest, local))]
    copies.append(
        pltpu.make_async_copy(coarse_ref.at[pl.ds(dev_ref[0] * tiles, tiles)], coarse_scr, in_sem.at[len(local)])
    )
    for copy in copies[:8]:
        copy.start()
    tile_copy(0).start()
    for copy in copies[8:]:
        copy.start()
    for t in range(1, tiles):
        tile_copy(t).start()
    copies[7].wait()
    want_vmem[...] = wanted_blocks(pick_scr[...], dev_ref[0], span_blocks)
    fetch = pltpu.make_async_copy(want_vmem, want_smem, want_sem)
    fetch.start()
    for copy in copies[:7]:
        copy.wait()
    rows = gain_scr[...]
    gain = jnp.concatenate([rows[k:k + 1, :] for k in range(rows.shape[0])], axis=1)
    gain_cols = jnp.broadcast_to(gain, (LANES, gain.shape[1])).T
    w_scr[:, 0:LANES] = (wq_scr[...].astype(F32) * gain_cols.astype(F32)).astype(BF16)
    gain = gain.astype(F32)
    scaled = lambda ref: (ref[...].astype(F32) * gain).astype(BF16)
    w_scr[:, LANES:2 * LANES] = jnp.concatenate([scaled(sk_scr), scaled(sv_scr)], axis=0).T
    w_scr[:, 2 * LANES:3 * LANES] = jnp.concatenate([scaled(ck_scr), scaled(cv_scr)], axis=0).T
    bw = scaled(bw_scr)
    pad = jnp.zeros((LANES - bw.shape[0], bw.shape[1]), BF16)
    w_scr[:, 3 * LANES:4 * LANES] = jnp.concatenate([bw, pad], axis=0).T
    for copy in copies[8:]:
        copy.wait()

    first_half = (lane % HEAD_DIM) < 32
    blocks = TILE // CMP_BLOCK
    low_b = lax.broadcasted_iota(jnp.int32, (blocks, LANES), 1) < HEAD_DIM
    per = TILE // SEL_BLOCK

    def out_copies(t):
        at = pl.ds(pl.multiple_of(t * TILE, TILE), TILE)
        pairs = (
            (qp_scr.at[:, at, :], qp_ref.at[:, at, :]),
            (qt_scr.at[:, at, :], qt_ref.at[:, at, :]),
            (kv_scr.at[pl.ds(t * per, per)], kv_ref.at[pl.ds(t * per, per)]),
            (gc_scr.at[at, :], gc_ref.at[at, :]),
            (gs_scr.at[at, :], gs_ref.at[at, :]),
        )
        return [pltpu.make_async_copy(src, dst, out_sem.at[i]) for i, (src, dst) in enumerate(pairs)]

    def tile(step, carry):
        prev = jnp.maximum(step - 1, 0)
        now = jnp.minimum(step, tiles - 1)
        raw = raw_scr[...]
        inv = inv_scr[...]

        @pl.when(step < tiles)
        def _():
            tile_copy(now).wait()

        fresh = jnp.dot(tok_scr[now], w_scr[...], preferred_element_type=F32)
        squares = jnp.zeros((TILE, LANES), F32)
        for k in range(tok_scr.shape[2] // LANES):
            part = tok_scr[now, :, k * LANES:(k + 1) * LANES].astype(F32)
            squares = squares + part * part
        mean = jnp.sum(squares, axis=-1, keepdims=True) * (1.0 / tok_scr.shape[2])

        ch = coarse_scr[prev, 0:1, :]
        sh = coarse_scr[prev, 1:2, :]
        cl = fine_scr[0]
        sl = fine_scr[1]
        cosine = ch * cl - sh * sl
        sine = sh * cl + ch * sl

        def turn(v):
            swapped = jnp.where(first_half, pltpu.roll(v, LANES - 32, 1), pltpu.roll(v, 32, 1))
            return v * cosine + swapped * sine

        at = pl.ds(pl.multiple_of(prev * TILE, TILE), TILE)
        q = raw[:, 0:LANES] * (inv * (HEAD_DIM ** (-0.5) * LOG2E))
        turned = turn(q)
        qp_scr[0, at, :] = jnp.where(low, q, 0.0).astype(BF16)
        qp_scr[1, at, :] = jnp.where(low, pltpu.roll(q, HEAD_DIM, 1), 0.0).astype(BF16)
        qt_scr[0, at, :] = jnp.where(low, turned, 0.0).astype(BF16)
        qt_scr[1, at, :] = jnp.where(low, pltpu.roll(turned, HEAD_DIM, 1), 0.0).astype(BF16)
        kv = raw[:, LANES:2 * LANES] * inv
        kv = jnp.where(low, turn(kv), kv).astype(BF16)
        kv_scr[pl.ds(prev * per, per)] = kv.reshape(per, SEL_BLOCK, LANES)
        c_scr[...] = (raw[:, 2 * LANES:3 * LANES] * inv).astype(BF16).astype(F32)
        logits = pltpu.roll(raw[:, 3 * LANES:4 * LANES] * inv, LANES - tp_ref[0] * 2, 1)
        gates = 1.0 / (1.0 + jnp.exp(-logits))
        gc_scr[at, :] = jnp.where(low, gates[:, 0:1], gates[:, 1:2])
        gs_scr[at, :] = jnp.where(low, gates[:, 16:17], gates[:, 17:18])

        embed = jnp.concatenate([ke_scr[...], ve_scr[...]], axis=1).astype(F32)
        part = pl.ds(pl.multiple_of(prev * blocks, blocks), blocks)
        for pair in range(CMP_BLOCK // 2):
            r = 2 * pair
            a = c_scr[pl.ds(r, blocks, stride=CMP_BLOCK), :] + embed[r:r + 1, :]
            b = c_scr[pl.ds(r + 1, blocks, stride=CMP_BLOCK), :] + embed[r + 1:r + 2, :]
            cols = slice(pair * LANES, (pair + 1) * LANES)
            xk_scr[part, cols] = jnp.where(low_b, a, pltpu.roll(b, HEAD_DIM, 1))
            xv_scr[part, cols] = jnp.where(low_b, pltpu.roll(a, HEAD_DIM, 1), b)
        raw_scr[...] = fresh
        inv_scr[...] = lax.rsqrt(mean + NORM_EPS)

        @pl.when(step > 0)
        def _():
            for copy in out_copies(prev):
                copy.start()

        return carry

    lax.fori_loop(0, tiles + 1, tile, 0)
    fetch.wait()
    hidden_k = jax.nn.gelu(dot_nt(xk_scr[...].astype(BF16), ki_scr[...])).astype(BF16)
    hidden_v = jax.nn.gelu(dot_nt(xv_scr[...].astype(BF16), vi_scr[...])).astype(BF16)
    summary = jnp.concatenate(
        [
            jnp.dot(hidden_k, ko_scr[...], preferred_element_type=F32),
            jnp.dot(hidden_v, vo_scr[...], preferred_element_type=F32),
        ],
        axis=1,
    ).astype(BF16)

    def fill(d, carry):
        for j in range(half):
            first_scr[d, j] = kv_scr[want_smem[0, d * 2 * half + 2 * j]]
        first_scr[d, half] = summary
        pltpu.make_async_copy(first_scr.at[d], first_ref.at[d], out_sem.at[5]).start()
        return carry

    lax.fori_loop(0, owners, fill, 0)
    pairs = (
        (qp_scr, qp_ref), (qt_scr, qt_ref), (kv_scr, kv_ref), (gc_scr, gc_ref), (gs_scr, gs_ref),
        (first_scr, first_ref),
    )
    for i, (src, dst) in enumerate(pairs):
        pltpu.make_async_copy(src, dst, out_sem.at[i]).wait()


def pack_kernel(dev_ref, pick_ref, kv_ref, out_ref, out_scr, want_vmem, want_smem, want_sem, out_sem):
    want_vmem[...] = wanted_blocks(pick_ref[...], dev_ref[0], kv_ref.shape[0])
    fetch = pltpu.make_async_copy(want_vmem, want_smem, want_sem)
    fetch.start()
    fetch.wait()
    owners, half = out_scr.shape[:2]

    def fill(d, carry):
        for j in range(half):
            out_scr[d, j] = kv_ref[want_smem[0, d * 2 * half + 2 * j + 1]]
        pltpu.make_async_copy(out_scr.at[d], out_ref.at[d], out_sem).start()
        return carry

    lax.fori_loop(0, owners, fill, 0)
    pltpu.make_async_copy(out_scr, out_ref, out_sem).wait()


def heads_to_lanes(out):
    rows = out.shape[1] // 2
    return jnp.concatenate([out[:, :rows], out[:, rows:]], axis=0).T


def compress_kernel(dev_ref, qp_ref, sum_ref, gc_ref, out_ref, k_scr, v_scr):
    owners, _, blocks, _ = sum_ref.shape
    count = owners * blocks
    dev = dev_ref[0]
    step = pl.program_id(0)

    @pl.when(step == 0)
    def _():
        lane = lax.broadcasted_iota(jnp.int32, (blocks, LANES), 1)
        for slot in range(owners):
            span = jnp.where(slot == 0, dev, jnp.where(slot == dev, 0, slot))
            rows = slice(slot * blocks, (slot + 1) * blocks)
            pair = sum_ref[span, 0].astype(F32)
            hide = jnp.where(span <= dev, 0.0, MASKED)
            k_scr[rows, :] = jnp.where(lane < HEAD_DIM, pair, jnp.where(lane == HEAD_DIM, hide, 0.0)).astype(BF16)
            v_scr[:, rows] = pair.T[HEAD_DIM:, :].astype(BF16)

    size = qp_ref.shape[1]
    lane = lax.broadcasted_iota(jnp.int32, (2 * size, LANES), 1)
    col = lax.broadcasted_iota(jnp.int32, (1, 2 * size), 1) % size
    own = lax.broadcasted_iota(jnp.int32, (blocks, 2 * size), 0)
    limit = (step * size + col + 1) // CMP_BLOCK
    q = qp_ref[...].reshape(2 * size, LANES)
    q = jnp.where(lane == HEAD_DIM, 1.0, q.astype(F32)).astype(BF16)
    scores = dot_nt(k_scr[...], q)
    near = jnp.where(own < limit, scores[:blocks], MASKED)
    scores = jnp.concatenate([near, scores[blocks:]], axis=0)
    top = jnp.max(scores, axis=0, keepdims=True)
    probs = jnp.exp2(scores - top)
    total = jnp.sum(probs, axis=0, keepdims=True)
    out = jnp.dot(v_scr[...], probs.astype(BF16), preferred_element_type=F32)
    out = jnp.where((limit > 0) | (dev > 0), out / total, 0.0)
    out_ref[...] = gc_ref[...] * heads_to_lanes(out)


def select_kernel(
    dev_ref, pick_ref, qt_ref, kv_ref, in_ref, gs_ref, cmp_ref, out_ref,
    q_scr, k_scr, gs_scr, cmp_scr, o_scr, pick_sem, sem, out_sem, *, parity
):
    count = out_ref.shape[0]
    dev = dev_ref[0]
    first = dev * 2 * count + parity

    def start(block, carry):
        for j in range(FAR_PICKS):
            span = pick_ref[j, first + 2 * block] // SPAN_BLOCKS
            rows = pl.ds(Q_BLOCK + j * SEL_BLOCK, SEL_BLOCK)
            pltpu.make_async_copy(in_ref.at[span, block], k_scr.at[block, rows, :], pick_sem.at[block]).start()
        return carry

    own_rows = k_scr.at[:, pl.ds(0, Q_BLOCK), :]
    early = [
        pltpu.make_async_copy(qt_ref.at[:, :, parity], q_scr, sem.at[0]),
        pltpu.make_async_copy(kv_ref.at[:, parity], own_rows, sem.at[1]),
    ]
    late = [
        pltpu.make_async_copy(gs_ref.at[:, parity], gs_scr, sem.at[2]),
        pltpu.make_async_copy(cmp_ref.at[:, parity], cmp_scr, sem.at[3]),
    ]
    for copy in early:
        copy.start()
    lax.fori_loop(0, count, start, 0)
    for copy in late:
        copy.start()
    for copy in early:
        copy.wait()
    low = lax.broadcasted_iota(jnp.int32, (Q_BLOCK, LANES), 1) < HEAD_DIM
    row = lax.broadcasted_iota(jnp.int32, (2 * Q_BLOCK, Q_BLOCK), 0) % Q_BLOCK
    causal = lax.broadcasted_iota(jnp.int32, (2 * Q_BLOCK, Q_BLOCK), 1) <= row
    far_keys = FAR_PICKS * SEL_BLOCK
    pick_of = lax.broadcasted_iota(jnp.int32, (1, far_keys), 1) // SEL_BLOCK
    low_k = lax.broadcasted_iota(jnp.int32, (Q_BLOCK + far_keys, LANES), 1) < HEAD_DIM

    def body(group, carry):
        scored = []
        for u in range(TOGETHER):
            block = group * TOGETHER + u
            far = k_scr.at[block, pl.ds(Q_BLOCK, far_keys), :]
            pltpu.make_async_copy(far, far, pick_sem.at[block]).wait()
        for u in range(TOGETHER):
            block = group * TOGETHER + u
            keys = k_scr[block]
            scored.append((block, keys, dot_nt(q_scr[:, block].reshape(2 * Q_BLOCK, LANES), keys)))
        weighed = []
        for block, keys, scores in scored:
            index = first + 2 * block
            bias = jnp.zeros((1, far_keys), F32)
            for j in range(FAR_PICKS):
                later = pick_ref[j, index] >= index * (Q_BLOCK // SEL_BLOCK)
                bias = jnp.where(pick_of == j, jnp.where(later, MASKED, 0.0), bias)
            own = jnp.where(causal, scores[:, :Q_BLOCK], MASKED)
            scores = jnp.concatenate([own, scores[:, Q_BLOCK:] + bias], axis=1)
            top = jnp.max(scores, axis=1, keepdims=True)
            weighed.append((block, keys, jnp.exp2(scores - top).astype(BF16)))

        @pl.when(group == 0)
        def _():
            for copy in late:
                copy.wait()

        for block, keys, probs in weighed:
            values = jnp.where(low_k, 1.0, keys.astype(F32)).astype(BF16)
            mixed = jnp.dot(probs, values, preferred_element_type=F32)
            out = mixed / pltpu.roll(mixed, HEAD_DIM, 1)
            joined = jnp.where(low, pltpu.roll(out[:Q_BLOCK], HEAD_DIM, 1), out[Q_BLOCK:])
            o_scr[block] = (cmp_scr[block] + gs_scr[block] * joined).astype(BF16)
            pltpu.make_async_copy(o_scr.at[block], out_ref.at[block], out_sem).start()
        return carry

    lax.fori_loop(0, count // TOGETHER, body, 0)
    pltpu.make_async_copy(o_scr, out_ref, out_sem).wait()


def whole(shape):
    return pl.BlockSpec(shape, lambda i, *_: (0,) * len(shape))


def per_device(
    tokens, norm_gain, query_weight, cmp_key_weight, cmp_value_weight, sel_key_weight, sel_value_weight,
    branch_weight, key_embed, key_inner, key_outer, value_embed, value_inner, value_outer, out_weight, chosen,
):
    tok_rows, width = tokens.shape
    owners = lax.axis_size("kv")
    dev = lax.axis_index("kv")
    tp = lax.axis_index("tp")
    span_queries = tok_rows // Q_BLOCK
    span_blocks = tok_rows // SEL_BLOCK
    cmp_blocks = tok_rows // CMP_BLOCK
    half = span_queries // 2
    picks = chosen[0].T
    dev = dev.astype(jnp.int32).reshape(1)
    tp = tp.astype(jnp.int32).reshape(1)

    coarse, fine = rope_tables(owners * tok_rows)
    steps = tok_rows // TILE
    gates_t = branch_weight.transpose(0, 2, 1).reshape(-1, width)
    slots = lambda n: jax.ShapeDtypeStruct((owners, n, SEL_BLOCK, LANES), BF16)
    inputs = [
        tokens, norm_gain.reshape(-1, LANES), query_weight, sel_key_weight.T, sel_value_weight.T,
        cmp_key_weight.T, cmp_value_weight.T, gates_t, picks, jnp.asarray(fine), jnp.asarray(coarse),
        key_embed[0], key_inner[0].T, key_outer[0], value_embed[0], value_inner[0].T, value_outer[0],
    ]
    outputs = [
        jax.ShapeDtypeStruct((2, tok_rows, LANES), BF16),
        jax.ShapeDtypeStruct((2, tok_rows, LANES), BF16),
        jax.ShapeDtypeStruct((span_blocks, SEL_BLOCK, LANES), BF16),
        jax.ShapeDtypeStruct((tok_rows, LANES), F32),
        jax.ShapeDtypeStruct((tok_rows, LANES), F32),
        slots(half + 1),
    ]
    local = [pltpu.VMEM(v.shape, v.dtype) for v in inputs]
    local[0] = pltpu.VMEM((steps, TILE, width), BF16)
    local[10] = pltpu.VMEM((steps, 2, LANES), F32)
    any_space = pl.BlockSpec(memory_space=pl.ANY)
    big = pltpu.CompilerParams(dimension_semantics=("arbitrary",), vmem_limit_bytes=67_043_328)
    qp, qt, kv, gate_cmp, gate_sel, first = pl.pallas_call(
        project_kernel,
        grid_spec=pltpu.PrefetchScalarGridSpec(
            num_scalar_prefetch=2,
            grid=(1,),
            in_specs=[any_space] * len(inputs),
            out_specs=[any_space] * len(outputs),
            scratch_shapes=[
                *local,
                *[pltpu.VMEM(v.shape, v.dtype) for v in outputs],
                pltpu.VMEM((width, 4 * LANES), BF16),
                pltpu.VMEM((TILE, 4 * LANES), F32),
                pltpu.VMEM((TILE, 1), F32),
                pltpu.VMEM((TILE, LANES), F32),
                pltpu.VMEM((cmp_blocks, CMP_BLOCK * HEAD_DIM), F32),
                pltpu.VMEM((cmp_blocks, CMP_BLOCK * HEAD_DIM), F32),
                pltpu.VMEM((1, picks.shape[1]), jnp.int32),
                pltpu.SMEM((1, picks.shape[1]), jnp.int32),
                pltpu.SemaphoreType.DMA((steps,)),
                pltpu.SemaphoreType.DMA((len(inputs) - 1,)),
                pltpu.SemaphoreType.DMA,
                pltpu.SemaphoreType.DMA((len(outputs),)),
            ],
        ),
        out_shape=outputs,
        compiler_params=big,
        name="project",
    )(dev, tp, *inputs)
    second = pl.pallas_call(
        pack_kernel,
        grid_spec=pltpu.PrefetchScalarGridSpec(
            num_scalar_prefetch=1,
            grid=(1,),
            in_specs=[whole(picks.shape), whole(kv.shape)],
            out_specs=any_space,
            scratch_shapes=[
                pltpu.VMEM((owners, half, SEL_BLOCK, LANES), BF16),
                pltpu.VMEM((1, picks.shape[1]), jnp.int32),
                pltpu.SMEM((1, picks.shape[1]), jnp.int32),
                pltpu.SemaphoreType.DMA,
                pltpu.SemaphoreType.DMA,
            ],
        ),
        out_shape=slots(half),
        compiler_params=big,
        name="pack",
    )(dev, picks, kv)
    first = lax.all_to_all(first, "kv", 0, 0, tiled=True)
    second = lax.all_to_all(second, "kv", 0, 0, tiled=True)

    gated = pl.pallas_call(
        compress_kernel,
        grid_spec=pltpu.PrefetchScalarGridSpec(
            num_scalar_prefetch=1,
            grid=(4,),
            in_specs=[
                pl.BlockSpec((2, tok_rows // 4, LANES), lambda i, *m: (0, i, 0)),
                pl.BlockSpec((owners, 1, cmp_blocks, LANES), lambda i, *m: (0, half, 0, 0)),
                pl.BlockSpec((tok_rows // 4, LANES), lambda i, *m: (i, 0)),
            ],
            out_specs=pl.BlockSpec((tok_rows // 4, LANES), lambda i, *m: (i, 0)),
            scratch_shapes=[
                pltpu.VMEM((owners * cmp_blocks, LANES), BF16),
                pltpu.VMEM((HEAD_DIM, owners * cmp_blocks), BF16),
            ],
        ),
        out_shape=jax.ShapeDtypeStruct((tok_rows, LANES), F32),
        compiler_params=pltpu.CompilerParams(
            dimension_semantics=("arbitrary",), vmem_limit_bytes=67_043_328
        ),
        name="compress",
    )(dev, qp, first, gate_cmp)

    by_parity = lambda v: v.reshape(half, 2, Q_BLOCK, LANES)

    def select(incoming, parity):
        return pl.pallas_call(
            functools.partial(select_kernel, parity=parity),
            grid_spec=pltpu.PrefetchScalarGridSpec(
                num_scalar_prefetch=2,
                grid=(1,),
                in_specs=[pl.BlockSpec(memory_space=pl.ANY)] * 5,
                out_specs=pl.BlockSpec(memory_space=pl.ANY),
                scratch_shapes=[
                    pltpu.VMEM((2, half, Q_BLOCK, LANES), BF16),
                    pltpu.VMEM((half, Q_BLOCK + FAR_PICKS * SEL_BLOCK, LANES), BF16),
                    pltpu.VMEM((half, Q_BLOCK, LANES), F32),
                    pltpu.VMEM((half, Q_BLOCK, LANES), F32),
                    pltpu.VMEM((half, Q_BLOCK, LANES), BF16),
                    pltpu.SemaphoreType.DMA((half,)),
                    pltpu.SemaphoreType.DMA((4,)),
                    pltpu.SemaphoreType.DMA,
                ],
            ),
            out_shape=jax.ShapeDtypeStruct((half, Q_BLOCK, LANES), BF16),
            compiler_params=pltpu.CompilerParams(
                dimension_semantics=("arbitrary",), vmem_limit_bytes=67_043_328
            ),
            name="select",
        )(
            dev, picks, qt.reshape(2, half, 2, Q_BLOCK, LANES), by_parity(kv), incoming,
            by_parity(gate_sel), by_parity(gated),
        )

    outs = []
    for incoming, parity in ((first, 0), (second, 1)):
        mixed = select(incoming, parity)
        rows = lax.all_to_all(mixed, "tp", 0, 0, tiled=True)
        weight = out_weight.reshape(rows.shape[0], LANES, out_weight.shape[1])
        outs.append(jnp.einsum("trc,tcd->rd", rows, weight, preferred_element_type=F32).astype(BF16))
    return jnp.concatenate(outs, axis=0)


def solution(mesh):
    placed = (
        P("kv", None),
        P(),
        P(None, "tp"),
        P(None, "tp"),
        P(None, "tp"),
        P(None, "tp"),
        P(None, "tp"),
        P(),
        P("tp", None, None),
        P("tp", None, None),
        P("tp", None, None),
        P("tp", None, None),
        P("tp", None, None),
        P("tp", None, None),
        P(),
        P("tp", None, None),
    )
    return jax.shard_map(
        per_device, mesh=mesh, in_specs=placed, out_specs=P(("kv", "tp"), None), check_vma=False
    )
```

time: 142 us -> 122 us (0.86)
  waiting for transfers between devices: 3.98 us -> 50.1 us
  blocking collectives: 38.9 us -> 0 us
  local copies, waits for them, and re-layouts: 25.7 us -> 0 us
  starting transfers between devices: 17.3 us -> 25.7 us
  Pallas kernels: 46.8 us -> 38.5 us
    all_to_all x1 -> x0, blocking collectives: 38.9 us -> none  [per_device(): first = lax.all_to_all(first, 'kv', 0, 0, tiled=True)]
    all_to_all x0 -> x1, waiting for transfers between devices: none -> 31.9 us  [per_device(): first = lax.all_to_all(first, 'kv', 0, 0, tiled=True)]
    unnamed x54 -> x0, local copies, waits for them, and re-layouts: 24.6 us -> none
    all_to_all x1, waiting for transfers between devices: 0.51 us -> 13.8 us  [per_device(): second = lax.all_to_all(second, 'kv', 0, 0, tiled=True)]
    all_to_all x0 -> x1, starting transfers between devices: none -> 8.46 us  [per_device(): first = lax.all_to_all(first, 'kv', 0, 0, tiled=True)]
    pallas_call x2, Pallas kernels: 17.4 us -> 11.2 us  [select(): pl.pallas_call(functools.partial(select_kernel, parity=parity), grid_spec...]
    pallas_call x1, Pallas kernels: 12.5 us -> 8.67 us  [per_device(): pl.pallas_call(compress_kernel, grid_spec=pltpu.PrefetchScalarGridSpec(nu...]
    pallas_call x0 -> x1, Pallas kernels: none -> 2.98 us  [per_device(): pl.pallas_call(pack_kernel, grid_spec=pltpu.PrefetchScalarGridSpec(num_sc...]
  transfers between devices with their start and end apart: 3 -> 4, of which waited for: 2 -> 4; matrix products, arithmetic and copies ran while one was open for 2% -> 2% of each run, Pallas kernels for 21% -> 19%
where the time goes in v2:
time: 122 us; the launch traced here: 121 us
  waiting for transfers between devices  50.1 us (41%)
  Pallas kernels  38.5 us (32%)
  starting transfers between devices  25.7 us (21%)
  matrix products  5.9 us (5%)
    all_to_all x1, waiting for transfers between devices, per_device(): first = lax.all_to_all(first, 'kv', 0, 0, tiled=True)  31.9 us
    pallas_call x1, Pallas kernels, per_device(): pl.pallas_call(project_kernel, grid_spec=pltpu.PrefetchScalarGridSpec(num...  15.7 us
    all_to_all x1, waiting for transfers between devices, per_device(): second = lax.all_to_all(second, 'kv', 0, 0, tiled=True)  13.8 us
    all_to_all x2, starting transfers between devices, per_device(): rows = lax.all_to_all(mixed, 'tp', 0, 0, tiled=True)  12.8 us
    pallas_call x2, Pallas kernels, select(): pl.pallas_call(functools.partial(select_kernel, parity=parity), grid_spec...  11.2 us
    pallas_call x1, Pallas kernels, per_device(): pl.pallas_call(compress_kernel, grid_spec=pltpu.PrefetchScalarGridSpec(nu...  8.67 us
    all_to_all x1, starting transfers between devices, per_device(): first = lax.all_to_all(first, 'kv', 0, 0, tiled=True)  8.46 us
    dot_general x2, matrix products, per_device(): jnp.einsum('trc,tcd->rd', rows, weight, preferred_element_type=F32)  5.9 us
  transfers between devices with their start and end apart: 4, of which 4 were waited for; matrix products, arithmetic and copies ran while one was open for 2% of the time, Pallas kernels for 19%

profile of v2, /device:TPU:1, one launch (start us, length us, event | category | flops | bytes accessed | tf_op | source)
XLA Modules:
  0.0 121.4 jit_solution(16106504867713239113)
XLA Ops:
  0.0 15.7 %project.1 = (bf16[2,2048,128]{2,1,0:T(8,128)(2,1)}, bf16[2,2048,128]{2,1,0:T(8,128)(2,1)}, bf16[32,64,128]{2,1,0:T(8,128)(2,1)}, f32[2048,128]{1,0:T(8,128)}, f...) custom-call(s32[1]{0:T(128)} %bitcast.dev_ref, s32[1]{0:T(128)} %bitcast.3.tp_ref, bf16[2048,2048]{1,0:T(8,128)(2,1)} %refs_0_.1, ...), custom_call_target="tpu_custom_call" | custom-call | tf_op jit(solution)/shard_map/project/pallas_call | solution.py:388
  15.7 8.5 %all-to-all-start = ((bf16[16,9,64,128]{3,2,1,0:T(8,128)(2,1)}), bf16[16,9,64,128]{3,2,1,0:T(8,128)(2,1)}, u32[]{:S(2)}, u32[]{:S(2)}) async-start(bf16[16,9,64,128]{3,2,1,0:T(8,128)(2,1)} %get-tuple-element.13), calls=%async_computation | async-start | bytes 4718592 | tf_op jit(solution)/shard_map/all_to_all | solution.py:435
  24.1 3.0 %pack.1 = bf16[16,8,64,128]{3,2,1,0:T(8,128)(2,1)} custom-call(s32[1]{0:T(128)} %bitcast.dev_ref, s32[8,256]{1,0:T(8,128)} %bitcast.58, bf16[32,64,128]{2,1,0:T(8,128)(2,1)} %get-tuple-element.12.kv_ref), custom_call_target="tpu_custom_call" | custom-call | tf_op jit(solution)/shard_map/pack/pallas_call | solution.py:416
  27.1 31.9 %all-to-all-done.sum_ref.in_ref = bf16[16,9,64,128]{3,2,1,0:T(8,128)(2,1)} async-done(((bf16[16,9,64,128]{3,2,1,0:T(8,128)(2,1)}), bf16[16,9,64,128]{3,2,1,0:T(8,128)(2,1)}, u32[]{:S(2)}, u32[]{:S(2)}) %all-to-all-start) | async-done | bytes 2359328 | tf_op jit(solution)/shard_map/all_to_all | solution.py:435
  59.0 4.4 %all-to-all-start.2 = ((bf16[16,8,64,128]{3,2,1,0:T(8,128)(2,1)}), bf16[16,8,64,128]{3,2,1,0:T(8,128)(2,1)}, u32[]{:S(2)}, u32[]{:S(2)}) async-start(bf16[16,8,64,128]{3,2,1,0:T(8,128)(2,1)} %pack.1), calls=%async_computation.2 | async-start | bytes 4194304 | tf_op jit(solution)/shard_map/all_to_all | solution.py:436
  63.4 8.7 %compress.1 = f32[2048,128]{1,0:T(8,128)} custom-call(s32[1]{0:T(128)} %bitcast.dev_ref, bf16[2,2048,128]{2,1,0:T(8,128)(2,1)} %get-tuple-element.15.qp_ref, bf16[16,9,64,128]{3,2,1,0:T(8,128)(2,1)} %all-to-all-done.sum_ref.in_ref, f32[2048,128]{1,0:T(8,128)} %get-tuple-element.16.gc_ref), custom_call_target="tpu_custom_call" | custom-call | tf_op jit(solution)/shard_map/compress/pallas_call | solution.py:438
  72.1 5.6 %select.2 = bf16[8,128,128]{2,1,0:T(8,128)(2,1)} custom-call(s32[1]{0:T(128)} %bitcast.dev_ref, s32[8,256]{1,0:T(8,128)} %bitcast.59, bf16[2,8,2,128,128]{4,3,2,1,0:T(8,128)(2,1)} %bitcast.46, bf16[8,2,128,128]{3,2,1,0:T(8,128)(2,1)} %bitcast.44, bf16[16,9,64,128]{3,2,1,0:T(8,128)(2,1)} %all-to-all-done.sum_ref.in_ref, f32[8,2,128,128]{3,2,1,0:T(8,128)} %bitcast.48, ...), custom_call_target="tpu_custom_call" | custom-call | tf_op jit(solution)/shard_map/select/pallas_call | solution.py:464
  77.7 13.8 %all-to-all-done.2.in_ref = bf16[16,8,64,128]{3,2,1,0:T(8,128)(2,1)} async-done(((bf16[16,8,64,128]{3,2,1,0:T(8,128)(2,1)}), bf16[16,8,64,128]{3,2,1,0:T(8,128)(2,1)}, u32[]{:S(2)}, u32[]{:S(2)}) %all-to-all-start.2) | async-done | bytes 2097184 | tf_op jit(solution)/shard_map/all_to_all | solution.py:436
  91.5 8.4 %all-to-all-start.1 = ((bf16[8,128,128]{2,1,0:T(8,128)(2,1)}), bf16[8,128,128]{2,1,0:T(8,128)(2,1)}, u32[]{:S(2)}, u32[]{:S(2)}) async-start(bf16[8,128,128]{2,1,0:T(8,128)(2,1)} %select.2), calls=%async_computation.1 | async-start | bytes 524288 | tf_op jit(solution)/shard_map/all_to_all | solution.py:495
  100.0 5.6 %select.3 = bf16[8,128,128]{2,1,0:T(8,128)(2,1)} custom-call(s32[1]{0:T(128)} %bitcast.dev_ref, s32[8,256]{1,0:T(8,128)} %bitcast.60, bf16[2,8,2,128,128]{4,3,2,1,0:T(8,128)(2,1)} %bitcast.47, bf16[8,2,128,128]{3,2,1,0:T(8,128)(2,1)} %bitcast.45, bf16[16,8,64,128]{3,2,1,0:T(8,128)(2,1)} %all-to-all-done.2.in_ref, f32[8,2,128,128]{3,2,1,0:T(8,128)} %bitcast.49, ...), custom_call_target="tpu_custom_call" | custom-call | tf_op jit(solution)/shard_map/select/pallas_call | solution.py:464
  105.6 0.9 all-to-all-done.1
  106.5 4.4 %all-to-all-start.3 = ((bf16[8,128,128]{2,1,0:T(8,128)(2,1)}), bf16[8,128,128]{2,1,0:T(8,128)(2,1)S(1)}, u32[]{:S(2)}, u32[]{:S(2)}) async-start(bf16[8,128,128]{2,1,0:T(8,128)(2,1)} %select.3), calls=%async_computation.3 | async-start | bytes 524288 | tf_op jit(solution)/shard_map/all_to_all | solution.py:495
  110.9 3.0 %fusion = bf16[128,2048]{1,0:T(8,128)(2,1)S(1)} fusion(bf16[8,128,128]{2,1,0:T(8,128)(2,1)} %all-to-all-done.1, bf16[8,128,2048]{2,1,0:T(8,128)(2,1)} %bitcast.40), kind=kOutput, calls=%fused_computation.2 | convolution fusion | flops 537133056 | bytes 4980736 | tf_op jit(solution)/shard_map/trc,tcd->rd/dot_general | solution.py:497
  113.9 3.5 %all-to-all-done.3 = bf16[8,128,128]{2,1,0:T(8,128)(2,1)S(1)} async-done(((bf16[8,128,128]{2,1,0:T(8,128)(2,1)}), bf16[8,128,128]{2,1,0:T(8,128)(2,1)S(1)}, u32[]{:S(2)}, u32[]{:S(2)}) %all-to-all-start.3) | async-done | bytes 262176 | tf_op jit(solution)/shard_map/all_to_all | solution.py:495
  117.4 2.9 %fusion.1 = bf16[128,2048]{1,0:T(8,128)(2,1)S(1)} fusion(bf16[8,128,128]{2,1,0:T(8,128)(2,1)S(1)} %all-to-all-done.3, bf16[8,128,2048]{2,1,0:T(8,128)(2,1)} %bitcast.41), kind=kOutput, calls=%fused_computation.3 | convolution fusion | flops 537133056 | bytes 4980736 | tf_op jit(solution)/shard_map/trc,tcd->rd/dot_general | solution.py:497
  120.3 1.1 pad_maximum_fusion
Async XLA Ops:
  15.7 43.3 %all-to-all-start = ((bf16[16,9,64,128]{3,2,1,0:T(8,128)(2,1)}), bf16[16,9,64,128]{3,2,1,0:T(8,128)(2,1)}, u32[]{:S(2)}, u32[]{:S(2)}) async-start(bf16[16,9,64,128]{3,2,1,0:T(8,128)(2,1)} %get-tuple-element.13), calls=%async_computation | async-start | bytes 4718592 | tf_op jit(solution)/shard_map/all_to_all | solution.py:435
  59.0 32.5 %all-to-all-start.2 = ((bf16[16,8,64,128]{3,2,1,0:T(8,128)(2,1)}), bf16[16,8,64,128]{3,2,1,0:T(8,128)(2,1)}, u32[]{:S(2)}, u32[]{:S(2)}) async-start(bf16[16,8,64,128]{3,2,1,0:T(8,128)(2,1)} %pack.1), calls=%async_computation.2 | async-start | bytes 4194304 | tf_op jit(solution)/shard_map/all_to_all | solution.py:436
  91.5 15.0 %all-to-all-start.1 = ((bf16[8,128,128]{2,1,0:T(8,128)(2,1)}), bf16[8,128,128]{2,1,0:T(8,128)(2,1)}, u32[]{:S(2)}, u32[]{:S(2)}) async-start(bf16[8,128,128]{2,1,0:T(8,128)(2,1)} %select.2), calls=%async_computation.1 | async-start | bytes 524288 | tf_op jit(solution)/shard_map/all_to_all | solution.py:495
  106.5 10.9 %all-to-all-start.3 = ((bf16[8,128,128]{2,1,0:T(8,128)(2,1)}), bf16[8,128,128]{2,1,0:T(8,128)(2,1)S(1)}, u32[]{:S(2)}, u32[]{:S(2)}) async-start(bf16[8,128,128]{2,1,0:T(8,128)(2,1)} %select.3), calls=%async_computation.3 | async-start | bytes 524288 | tf_op jit(solution)/shard_map/all_to_all | solution.py:495
